TPU v7x, 512 devices: a whole 4x4x16 slice. The times are simulated.
512 devices in a mesh: sp: 32 (over z, core), tp: 16 (over y, x).
Axes of the slice: x: 4, y: 4, z: 16, core: 2. Of those that a mesh axis runs over, the one named last changes fastest.
Arguments:
- resid: bfloat16 [8192, 2048], P('sp'), may hold values from -18 to 18
- narrow_head_input: bfloat16 [8192, 1024], P('sp', 'tp'), may hold values from -6 to 6
- wide_head_input: bfloat16 [8192, 2048], P('sp', 'tp'), may hold values from -6 to 6
- key_group_input: bfloat16 [8192, 512], P('sp'), may hold values from -6 to 6
- query_group_input: bfloat16 [8192, 512], P('sp'), may hold values from -6 to 6
- narrow_output_gate: bfloat16 [8192, 1024], P('sp', 'tp'), may hold values from -6 to 6
- wide_output_gate: bfloat16 [8192, 2048], P('sp', 'tp'), may hold values from -6 to 6
- step_input_rows: bfloat16 [8192, 2, 16], P('sp', None, 'tp'), may hold values from -4 to 4
- head_decay_logarithm: float32 [2, 16], P(None, 'tp'), may hold values from -14 to -2
- position_log_decay: float32 [8192, 2, 16], P('sp', None, 'tp'), may hold values from -1.4 to 0
- direct_input_weight: float32 [2, 16], P(None, 'tp'), may hold values from 0.5 to 2
- narrow_conv_taps: float32 [4, 1024], P(None, 'tp'), may hold values from -3 to 3
- wide_conv_taps: float32 [4, 2048], P(None, 'tp'), may hold values from -3 to 3
- key_conv_taps: float32 [4, 512], replicated, may hold values from -3 to 3
- query_conv_taps: float32 [4, 512], replicated, may hold values from -3 to 3
- narrow_norm_gain: float32 [1024], P('tp'), may hold values from 0.1 to 1.9
- wide_norm_gain: float32 [2048], P('tp'), may hold values from 0.1 to 1.9
- narrow_output_rows: bfloat16 [1024, 2048], P('tp'), may hold values from -0.109375 to 0.109375
- wide_output_rows: bfloat16 [2048, 2048], P('tp'), may hold values from -0.109375 to 0.109375
- feedforward_norm_gain: float32 [2048], replicated, may hold values from 0.1 to 1.9
- routes: int32 [8192, 3], P('sp'), may hold values from 0 to 31, all different within a row; in each aligned block of 256 rows (0 to 255, 256 to 511, ...) at most 32 rows name the same one
- routing_weight_values: float32 [8192, 3], P('sp'), may hold values from 0.1 to 1
- expert_gate_matrix: bfloat16 [32, 2048, 2048], P('sp', None, 'tp'), may hold values from -1 to 1
- expert_up_matrix: bfloat16 [32, 2048, 2048], P('sp', None, 'tp'), may hold values from -1 to 1
- expert_down_matrix: bfloat16 [32, 2048, 2048], P('sp', 'tp'), may hold values from -0.015625 to 0.015625
Outputs:
- layer_out: bfloat16 [8192, 2048], P('sp', 'tp')
Inputs may be any that keep to these rules, and one draw needn't show every extreme that they name: `routes`: each token names 3 different experts. Among the tokens of one index of sp (aligned blocks of 256 rows) no expert is named by more than 32 of them, and in some blocks one is named by exactly 32.
All inputs are finite; a program needn't handle non-finite values.
Results may differ from a plain program's by a relative error of at most 0.015.
Values may be sent and summed in bfloat16 or wider, within the bound.
A program may use at most 64 MiB of HBM per device.

v0:
```python
import functools

import jax
import jax.numpy as jnp
from jax import lax
from jax.sharding import Mesh
from jax.sharding import PartitionSpec as P

HEADS = 16
NARROW_HEAD_DIM = 64
WIDE_HEAD_DIM = 128
GROUPS = 4
BLOCK = 128
SP = ("sp_0", "sp_1")


NORM_EPS = 1e-06
CLAMP_LIMIT = 7.0
SIGMOID_SCALE = 1.702
FULL_PRECISION = lax.Precision.HIGHEST


def passed_along(block, axis, distance):
    devices = range(lax.axis_size(axis))
    route = [(i - distance, i) for i in devices if i - distance in devices]
    return lax.ppermute(block, axis, route)


def filled_with(x, identity):
    return jax.tree.map(
        lambda part, zero: jnp.zeros_like(part) + jnp.asarray(zero, part.dtype), x, identity
    )


def all_in_one(x, axis):
    leaves = jax.tree.leaves(x)
    turns = sorted(range(len(leaves)), key=lambda k: -leaves[k].size)
    width = (1, *leaves[turns[0]].shape)[-1]
    lines = [
        jnp.pad(leaves[k].reshape(-1), (0, -leaves[k].size % width)).reshape(-1, width)
        for k in turns
    ]
    both, at, found = (lax.all_gather(jnp.concatenate(lines), axis), 0, {})
    for k, line in zip(turns, lines):
        piece = both[:, at : at + len(line)].reshape(len(both), -1)
        found[k] = piece[:, : leaves[k].size].reshape(-1, *leaves[k].shape)
        at += len(line)
    numbers = iter(range(len(leaves)))
    return jax.tree.map(lambda _: found[next(numbers)], x)


def entering_2(x, axes, combine, identity):
    before = start = filled_with(x, identity)
    running = x
    for axis in reversed(axes):
        length, mine = (lax.axis_size(axis), lax.axis_index(axis))
        pieces = all_in_one(
            jax.tree.map(
                lambda part, kind: part.astype(kind),
                running,
                jax.tree.map(lambda a: jnp.bfloat16 if a.dtype == jnp.float32 else a.dtype, x),
            ),
            axis,
        )
        inside, running = (start, start)
        for k in range(length):
            passed = k < mine
            running = combine(
                running, jax.tree.map(lambda part, own: part[k].astype(own.dtype), pieces, x)
            )
            inside = jax.tree.map(lambda new, old: jnp.where(passed, new, old), running, inside)
        before = combine(inside, before)
    return before


def split_up(x, dim, length):
    lengths = x.shape
    parts = x.reshape(*lengths[:dim], length, lengths[dim] // length, *lengths[dim + 1 :])
    return jnp.moveaxis(parts, dim, 0)


def sent_and_summed(x, axis, dim):
    length = lax.axis_size(axis)
    parts = lax.all_to_all(split_up(x, dim, length), axis, 0, 0, tiled=True)
    return jnp.sum(parts.astype(jnp.float32), axis=0)


def padded_to(lines, length):
    spare = -len(lines) % length
    return jnp.pad(lines, [(0, spare)] + [(0, 0)] * (lines.ndim - 1))


def in_order(parts, dim):
    parts = jnp.moveaxis(parts, 0, dim)
    lengths = parts.shape
    return parts.reshape(*lengths[:dim], lengths[dim] * lengths[dim + 1], *lengths[dim + 2 :])


def from_everyone(x, axis):
    copies = jnp.broadcast_to(x, (lax.axis_size(axis), *x.shape))
    return lax.all_to_all(copies, axis, split_axis=0, concat_axis=0, tiled=True)


def collect(x, axis, dim):
    return in_order(from_everyone(x, axis), dim)


def total_of(x, axes):
    lines = x.reshape(-1, x.shape[-1])
    own = sent_and_summed(padded_to(lines, lax.axis_size(axes)), axes, 0)
    whole = collect(own.astype(jnp.bfloat16), axes, 0)
    return whole[: len(lines)].reshape(x.shape).astype(jnp.float32)


def conv_with_rim(values, rim_rows, weight):
    length = values.shape[0]
    padded = jnp.concatenate([rim_rows, values], axis=0).astype(jnp.float32)
    accumulated = jnp.zeros((length, values.shape[1]), jnp.float32)
    for tap_index in range(weight.shape[0]):
        accumulated = accumulated + weight[tap_index] * padded[tap_index : tap_index + length]
    return jax.nn.silu(accumulated)


def pick_groups(channel_table, first_head, head_count):
    length = channel_table.shape[0]
    grouped = channel_table.reshape(length, GROUPS, -1)
    owners = (first_head + jnp.arange(head_count, dtype=jnp.int32)) // (HEADS // GROUPS)
    chooser = (owners[:, None] == jnp.arange(GROUPS, dtype=jnp.int32)[None, :]).astype(jnp.float32)
    return jnp.einsum("sgn,hg->shn", grouped, chooser, precision=FULL_PRECISION)


def local_head(values, step_logarithm, key_head_rows, query_head_rows, block_len):
    block_count = values.shape[0] // block_len
    values = values.reshape(block_count, block_len, -1)
    step_logarithm = step_logarithm.reshape(block_count, block_len)
    key_head_rows = key_head_rows.reshape(block_count, block_len, -1)
    query_head_rows = query_head_rows.reshape(block_count, block_len, -1)
    cum_decay = jnp.cumsum(step_logarithm, axis=1)
    causal_mask = jnp.arange(block_len)[:, None] >= jnp.arange(block_len)[None, :]
    decay_gaps = jnp.where(causal_mask[None], cum_decay[:, :, None] - cum_decay[:, None, :], -1e30)
    scores = jnp.einsum(
        "bln,bsn->bls", query_head_rows, key_head_rows, precision=FULL_PRECISION
    ) * jnp.exp(decay_gaps)
    inside = jnp.einsum("bls,bsp->blp", scores, values, precision=FULL_PRECISION)
    tail_decay = jnp.exp(cum_decay[:, -1:] - cum_decay)
    states = jnp.einsum(
        "bln,blp->bnp", key_head_rows * tail_decay[..., None], values, precision=FULL_PRECISION
    )
    totals = cum_decay[:, -1]

    def walk(running, member):
        return (jnp.exp(member[1]) * running + member[0], running)

    closing, entering = lax.scan(walk, jnp.zeros(states.shape[1:], jnp.float32), (states, totals))
    before = jnp.cumsum(totals) - totals
    return (inside, entering, closing, jnp.sum(totals), before, cum_decay, query_head_rows)


def finish_head(inside, entering, before, cum_decay, query_blocks, carried):
    starting = entering + jnp.exp(before)[:, None, None] * carried[None]
    readout = jnp.einsum(
        "bln,bnp->blp",
        query_blocks * jnp.exp(cum_decay)[..., None],
        starting,
        precision=FULL_PRECISION,
    )
    return (inside + readout).reshape(-1, inside.shape[-1])


def group_out(scanned, mixed_input_rows, direct_input_term, gate_input_rows, norm_gain_vector):
    length, head_count, head_dimension = mixed_input_rows.shape
    gated = jax.nn.silu(gate_input_rows.astype(jnp.float32)).reshape(
        length, head_count, head_dimension
    )
    result = (scanned + direct_input_term[None, :, None] * mixed_input_rows) * gated
    result = result * lax.rsqrt(jnp.mean(result * result, axis=-1, keepdims=True) + NORM_EPS)
    return (result.reshape(length, head_count * head_dimension) * norm_gain_vector).astype(
        jnp.bfloat16
    )


def head_pieces_list(
    mixed_input_rows,
    step_length_values,
    decay_vector,
    position_decay_rows,
    key_head_rows,
    query_head_rows,
):
    step_logarithm = -jnp.exp(decay_vector)[None, :] * step_length_values + position_decay_rows
    values = mixed_input_rows * step_length_values[..., None]
    walker = functools.partial(local_head, block_len=BLOCK)
    return jax.vmap(walker, in_axes=(1, 1, 1, 1))(
        values, step_logarithm, key_head_rows, query_head_rows
    )


def finish_group(parts, carried_states):
    return jax.vmap(finish_head, in_axes=(0, 0, 0, 0, 0, 0), out_axes=1)(
        parts[0], parts[1], parts[4], parts[5], parts[6], carried_states
    )


def chain_combine(earlier, later):
    return (
        earlier[0] + later[0],
        earlier[1] + later[1],
        jnp.exp(later[0])[:, None, None] * earlier[2] + later[2],
        jnp.exp(later[1])[:, None, None] * earlier[3] + later[3],
    )


def local(
    resid,
    narrow_head_input,
    wide_head_input,
    key_group_input,
    query_group_input,
    narrow_output_gate,
    wide_output_gate,
    step_input_rows,
    head_decay_logarithm,
    position_log_decay,
    direct_input_weight,
    narrow_conv_taps,
    wide_conv_taps,
    key_conv_taps,
    query_conv_taps,
    narrow_norm_gain,
    wide_norm_gain,
    narrow_output_rows,
    wide_output_rows,
    feedforward_norm_gain,
    routes,
    routing_weight_values,
    expert_gate_matrix,
    expert_up_matrix,
    expert_down_matrix,
):
    length = resid.shape[0]
    head_count = narrow_head_input.shape[1] // NARROW_HEAD_DIM
    rim_len = narrow_conv_taps.shape[0] - 1
    rim_rows = passed_along(
        (
            narrow_head_input[length - rim_len :],
            wide_head_input[length - rim_len :],
            key_group_input[length - rim_len :],
            query_group_input[length - rim_len :],
        ),
        SP,
        1,
    )
    narrow_head_mix = conv_with_rim(narrow_head_input, rim_rows[0], narrow_conv_taps).reshape(
        length, head_count, NARROW_HEAD_DIM
    )
    wide_head_mix = conv_with_rim(wide_head_input, rim_rows[1], wide_conv_taps).reshape(
        length, head_count, WIDE_HEAD_DIM
    )
    first_head = lax.axis_index("tp") * head_count
    key_head_rows = pick_groups(
        conv_with_rim(key_group_input, rim_rows[2], key_conv_taps), first_head, head_count
    )
    query_head_rows = pick_groups(
        conv_with_rim(query_group_input, rim_rows[3], query_conv_taps), first_head, head_count
    )
    step_length_values = jax.nn.softplus(step_input_rows.astype(jnp.float32))
    narrow_parts = head_pieces_list(
        narrow_head_mix,
        step_length_values[:, 0],
        head_decay_logarithm[0],
        position_log_decay[:, 0],
        key_head_rows,
        query_head_rows,
    )
    wide_parts = head_pieces_list(
        wide_head_mix,
        step_length_values[:, 1],
        head_decay_logarithm[1],
        position_log_decay[:, 1],
        key_head_rows,
        query_head_rows,
    )
    summary = (narrow_parts[3], wide_parts[3], narrow_parts[2], wide_parts[2])
    carried = entering_2(
        summary,
        SP,
        chain_combine,
        (
            jnp.zeros_like(summary[0]),
            jnp.zeros_like(summary[1]),
            jnp.zeros_like(summary[2]),
            jnp.zeros_like(summary[3]),
        ),
    )
    narrow_carry, wide_carry = (carried[2], carried[3])
    narrow_head_output = group_out(
        finish_group(narrow_parts, narrow_carry),
        narrow_head_mix,
        direct_input_weight[0],
        narrow_output_gate,
        narrow_norm_gain,
    )
    wide_head_output = group_out(
        finish_group(wide_parts, wide_carry),
        wide_head_mix,
        direct_input_weight[1],
        wide_output_gate,
        wide_norm_gain,
    )
    partial_mix = jnp.dot(
        narrow_head_output, narrow_output_rows, preferred_element_type=jnp.float32
    )
    partial_mix = partial_mix + jnp.dot(
        wide_head_output, wide_output_rows, preferred_element_type=jnp.float32
    )
    mixed = total_of(partial_mix.astype(jnp.bfloat16), "tp")
    hidden_state = resid.astype(jnp.float32) + mixed
    normed = (
        hidden_state
        * lax.rsqrt(jnp.mean(hidden_state * hidden_state, axis=-1, keepdims=True) + NORM_EPS)
        * feedforward_norm_gain
    ).astype(jnp.bfloat16)
    experts = lax.axis_size(SP)
    picks = routes.shape[1]
    capacity = 4 * length * picks // (3 * experts)
    column_width = normed.shape[1] // lax.axis_size("tp")
    tp_index = lax.axis_index("tp")
    flat_routes = routes.reshape(-1)
    member_hits = (flat_routes[:, None] == jnp.arange(experts, dtype=jnp.int32)[None, :]).astype(
        jnp.int32
    )
    ranks = jnp.sum((jnp.cumsum(member_hits, axis=0) - member_hits) * member_hits, axis=1)
    slot_ids = flat_routes * capacity + ranks
    source_rows = (
        jnp.zeros((experts * capacity,), jnp.int32)
        .at[slot_ids]
        .set(jnp.arange(length * picks, dtype=jnp.int32) // picks)
    )
    occupied = jnp.zeros((experts * capacity,), jnp.int32).at[slot_ids].set(1)
    gate_weight = expert_gate_matrix[0]
    up_weight = expert_up_matrix[0]
    down_weight = expert_down_matrix[0]
    own_columns = lax.dynamic_slice_in_dim(normed, tp_index * column_width, column_width, 1)
    outgoing = jnp.where(
        occupied[:, None] > 0, own_columns[source_rows], jnp.zeros((), jnp.bfloat16)
    )
    arrived = lax.all_to_all(
        outgoing.reshape(experts, capacity, column_width),
        SP,
        split_axis=0,
        concat_axis=0,
        tiled=True,
    )
    slot_parts = arrived.reshape(experts * capacity, column_width)
    piece = collect(slot_parts, "tp", 1)
    gate_pre = jnp.dot(piece, gate_weight, preferred_element_type=jnp.float32)
    up_pre = jnp.dot(piece, up_weight, preferred_element_type=jnp.float32)
    clamped = jnp.minimum(gate_pre, CLAMP_LIMIT)
    act = (
        (jnp.clip(up_pre, -CLAMP_LIMIT, CLAMP_LIMIT) + 1.0)
        * clamped
        * jax.nn.sigmoid(SIGMOID_SCALE * clamped)
    ).astype(jnp.bfloat16)
    partial_out = jnp.dot(act, down_weight, preferred_element_type=jnp.float32)
    summed = sent_and_summed(
        partial_out.reshape(experts, capacity, -1).astype(jnp.bfloat16), "tp", 2
    )
    returned = lax.all_to_all(
        summed.astype(jnp.bfloat16), SP, split_axis=0, concat_axis=0, tiled=True
    )
    token_rows = returned.reshape(experts * capacity, -1)[slot_ids].reshape(length, picks, -1)
    combined = jnp.sum(token_rows.astype(jnp.float32) * routing_weight_values[..., None], axis=1)
    own_state = lax.dynamic_slice_in_dim(hidden_state, tp_index * column_width, column_width, 1)
    return (own_state + combined).astype(jnp.bfloat16)


def solution(mesh):
    finer = Mesh(mesh.devices.reshape(16, 2, mesh.shape["tp"]), ("sp_0", "sp_1", "tp"))
    return jax.shard_map(
        local,
        mesh=finer,
        in_specs=(
            P(SP, None),
            P(SP, "tp"),
            P(SP, "tp"),
            P(SP, None),
            P(SP, None),
            P(SP, "tp"),
            P(SP, "tp"),
            P(SP, None, "tp"),
            P(None, "tp"),
            P(SP, None, "tp"),
            P(None, "tp"),
            P(None, "tp"),
            P(None, "tp"),
            P(),
            P(),
            P("tp"),
            P("tp"),
            P("tp", None),
            P("tp", None),
            P(),
            P(SP, None),
            P(SP, None),
            P(SP, None, "tp"),
            P(SP, None, "tp"),
            P(SP, "tp", None),
        ),
        out_specs=P(SP, "tp"),
        check_vma=False,
    )
```

profile of v0, /device:TPU:6, one launch (start us, length us, event | category | flops | bytes accessed | tf_op | source)
XLA Modules:
  0.0 353.5 jit_solution(17980917119176715900)
XLA Ops:
  0.8 1.7 collective-permute-start.1
  3.2 4.1 %collective-permute-start.3 = (bf16[3,128]{1,0:T(4,128)(2,1)S(1)}, bf16[3,128]{1,0:T(4,128)(2,1)S(1)}, u32[]{:S(2)}, u32[]{:S(2)}) collective-permute-start(bf16[3,128]{1,0:T(4,128)(2,1)S(1)} %slice.526), channel_id=1, source_target_pairs={{0,16},{16,32},{32,48},{48,64},{64,80},{80,96},{96,112},{112,128},... | collective-permute-start | bytes 2312 | tf_op jit(solution)/shard_map/ppermute | solution.py:26
  8.1 1.9 collective-permute-start.2
  10.7 3.9 %collective-permute-start = (bf16[3,512]{1,0:T(4,128)(2,1)S(1)}, bf16[3,512]{1,0:T(4,128)(2,1)S(1)}, u32[]{:S(2)}, u32[]{:S(2)}) collective-permute-start(bf16[3,512]{1,0:T(4,128)(2,1)S(1)} %slice.491), channel_id=1, source_target_pairs={{0,16},{16,32},{32,48},{48,64},{64,80},{80,96},{96,112},{112,128},... | collective-permute-start | bytes 9224 | tf_op jit(solution)/shard_map/ppermute | solution.py:26
  15.3 0.9 fusion.105
  16.2 1.4 fusion.112
  19.6 0.8 slice_bitcast_fusion.3
  22.8 0.8 slice_bitcast_fusion.7
  25.2 0.9 fusion.106
  26.8 1.4 fusion.109
  28.8 1.3 pad_bitcast_fusion.2
  30.2 0.8 maximum_convert_fusion.3
  31.8 0.9 maximum_convert_fusion.2
  32.8 1.0 maximum_convert_fusion.1
  35.4 2.8 while.27
  38.6 2.9 while.26
  42.1 1.9 all-gather.2
  50.7 37.3 %all-gather.3 = bf16[16,194,128]{2,1,0:T(8,128)(2,1)S(1)} all-gather(bf16[1,194,128]{2,1,0:T(8,128)(2,1)S(1)} %maximum_bitcast_fusion.1), channel_id=3, replica_groups=mesh['sp_0'=16,'sp_1'=2,'tp'=16] {'sp_0'}, dimensions={0}, use_global_device_ids=true | all-gather | bytes 844288 | tf_op jit(solution)/shard_map/all_gather | solution.py:43
  109.4 1.2 fusion.31
  110.5 1.2 multiply_add_fusion
  111.8 1.4 fusion.5
  113.2 1.5 multiply_reduce_fusion.3
  126.1 1.0 fusion.24
  127.3 1.2 convolution_add_fusion.1
  129.5 1.1 fusion.44
  130.6 1.5 fusion
  132.1 7.6 %all-to-all-start = ((bf16[16,16,2048]{2,1,0:T(8,128)(2,1)}), bf16[16,16,2048]{2,1,0:T(8,128)(2,1)S(1)}, u32[]{:S(2)}, u32[]{:S(2)}) async-start(bf16[16,16,2048]{2,1,0:T(8,128)(2,1)} %bitcast.113), calls=%async_computation | async-start | bytes 2097152 | tf_op jit(solution)/shard_map/all_to_all | solution.py:84
  140.3 1.7 reduce-window.26
  142.3 7.7 %all-to-all-done = bf16[16,16,2048]{2,1,0:T(8,128)(2,1)S(1)} async-done(((bf16[16,16,2048]{2,1,0:T(8,128)(2,1)}), bf16[16,16,2048]{2,1,0:T(8,128)(2,1)S(1)}, u32[]{:S(2)}, u32[]{:S(2)}) %all-to-all-start) | async-done | bytes 1048608 | tf_op jit(solution)/shard_map/all_to_all | solution.py:84
  150.2 1.1 broadcast_in_dim.54
  151.3 6.6 %all-to-all-start.1 = ((bf16[16,16,2048]{2,1,0:T(8,128)(2,1)}), bf16[16,16,2048]{2,1,0:T(8,128)(2,1)S(1)}, u32[]{:S(2)}, u32[]{:S(2)}) async-start(bf16[16,16,2048]{2,1,0:T(8,128)(2,1)} %broadcast_in_dim.54), calls=%async_computation.1 | async-start | bytes 2097152 | tf_op jit(solution)/shard_map/all_to_all | solution.py:101
  158.3 3.4 scatter_custom_fusion.1
  161.7 3.6 %scatter_custom_fusion = s32[1024]{0:T(1024)S(1)} fusion(s32[768]{0:T(1024)S(1)} %fusion.80, s32[768]{0:T(1024)S(1)} %broadcast.659, s32[]{:T(128)} %constant.141.clone.1), kind=kCustom, calls=%fused_computation.195 | custom fusion | bytes 4100 | tf_op jit(solution)/shard_map/scatter | solution.py:339
  166.2 2.0 all-to-all-done.1
  168.7 1.3 copy-done.1
  170.1 3.2 gather_fusion
  173.5 31.6 %all_to_all.30 = bf16[32,32,128]{2,1,0:T(8,128)(2,1)S(1)} all-to-all(bf16[32,32,128]{2,1,0:T(8,128)(2,1)S(1)} %broadcast_select_fusion), channel_id=1, replica_groups=mesh['sp_0'=16,'sp_1'=2,'tp'=16] {'sp_0','sp_1'}, dimensions={0} | all-to-all | bytes 524288 | tf_op jit(solution)/shard_map/all_to_all | solution.py:347
  205.8 54.3 %all_to_all.31 = bf16[16,1024,128]{1,2,0:T(8,128)(2,1)S(1)} all-to-all(bf16[16,1024,128]{1,2,0:T(8,128)(2,1)S(1)} %broadcast_in_dim.60), channel_id=1, replica_groups=mesh['sp_0'=16,'sp_1'=2,'tp'=16] {'tp'}, dimensions={0} | all-to-all | bytes 8388608 | tf_op jit(solution)/shard_map/all_to_all | solution.py:101
  260.2 1.3 convolution_minimum_fusion
  261.5 1.3 fusion.4
  262.8 1.2 convert_bitcast_fusion
  264.0 1.1 copy.147
  265.1 53.2 %all_to_all.32 = bf16[16,32,32,128]{3,2,1,0:T(8,128)(2,1)} all-to-all(bf16[16,32,32,128]{3,2,1,0:T(8,128)(2,1)S(1)} %bitcast.275), channel_id=1, replica_groups=mesh['sp_0'=16,'sp_1'=2,'tp'=16] {'tp'}, dimensions={0} | all-to-all | bytes 8388608 | tf_op jit(solution)/shard_map/all_to_all | solution.py:84
  318.3 3.6 %reduce_sum.97 = bf16[32,32,128]{2,1,0:T(8,128)(2,1)} reduce(bf16[16,32,32,128]{3,2,1,0:T(8,128)(2,1)} %all_to_all.32, bf16[]{:T(256)} %constant.145.clone.1), dimensions={0}, to_apply=%region_19.20 | reduce | flops 1966080 | bytes 4456450 | tf_op jit(solution)/shard_map/reduce_sum | solution.py:85
  321.9 5.0 %all-to-all-start.5 = ((bf16[32,32,128]{2,1,0:T(8,128)(2,1)}), bf16[32,32,128]{2,1,0:T(8,128)(2,1)S(1)}, u32[]{:S(2)}, u32[]{:S(2)}) async-start(bf16[32,32,128]{2,1,0:T(8,128)(2,1)} %reduce_sum.97), calls=%async_computation.5 | async-start | bytes 524288 | tf_op jit(solution)/shard_map/all_to_all | solution.py:368
  327.0 22.5 %all-to-all-done.5 = bf16[32,32,128]{2,1,0:T(8,128)(2,1)S(1)} async-done(((bf16[32,32,128]{2,1,0:T(8,128)(2,1)}), bf16[32,32,128]{2,1,0:T(8,128)(2,1)S(1)}, u32[]{:S(2)}, u32[]{:S(2)}) %all-to-all-start.5) | async-done | bytes 262176 | tf_op jit(solution)/shard_map/all_to_all | solution.py:368
  349.5 1.9 gather_fusion.1
  352.0 1.6 add_convert_fusion
  (148 shorter events, 35.2 us)
Async XLA Ops:
  0.0 262.8 %copy-start = (bf16[1,128,2048]{2,1,0:T(8,128)(2,1)S(1)}, bf16[1,128,2048]{2,1,0:T(8,128)(2,1)}, u32[]{:S(2)}) copy-start(bf16[1,128,2048]{2,1,0:T(8,128)(2,1)} %param.53) | copy-start | bytes 1572868
  0.8 32.1 %collective-permute-start.1 = (bf16[3,512]{1,0:T(4,128)(2,1)S(1)}, bf16[3,512]{1,0:T(4,128)(2,1)S(1)}, u32[]{:S(2)}, u32[]{:S(2)}) collective-permute-start(bf16[3,512]{1,0:T(4,128)(2,1)S(1)} %slice.500), channel_id=1, source_target_pairs={{0,16},{16,32},{32,48},{48,64},{64,80},{80,96},{96,112},{112,128},... | collective-permute-start | bytes 9224 | tf_op jit(solution)/shard_map/ppermute | solution.py:26
  3.2 28.6 %collective-permute-start.3 = (bf16[3,128]{1,0:T(4,128)(2,1)S(1)}, bf16[3,128]{1,0:T(4,128)(2,1)S(1)}, u32[]{:S(2)}, u32[]{:S(2)}) collective-permute-start(bf16[3,128]{1,0:T(4,128)(2,1)S(1)} %slice.526), channel_id=1, source_target_pairs={{0,16},{16,32},{32,48},{48,64},{64,80},{80,96},{96,112},{112,128},... | collective-permute-start | bytes 2312 | tf_op jit(solution)/shard_map/ppermute | solution.py:26
  8.1 22.1 %collective-permute-start.2 = (bf16[3,64]{0,1:T(8,128)(2,1)S(1)}, bf16[3,64]{0,1:T(8,128)(2,1)S(1)}, u32[]{:S(2)}, u32[]{:S(2)}) collective-permute-start(bf16[3,64]{0,1:T(8,128)(2,1)S(1)} %slice.512), channel_id=1, source_target_pairs={{0,16},{16,32},{32,48},{48,64},{64,80},{80,96},{96,112},{112,128},... | collective-permute-start | bytes 1160 | tf_op jit(solution)/shard_map/ppermute | solution.py:26
  10.7 97.0 %collective-permute-start = (bf16[3,512]{1,0:T(4,128)(2,1)S(1)}, bf16[3,512]{1,0:T(4,128)(2,1)S(1)}, u32[]{:S(2)}, u32[]{:S(2)}) collective-permute-start(bf16[3,512]{1,0:T(4,128)(2,1)S(1)} %slice.491), channel_id=1, source_target_pairs={{0,16},{16,32},{32,48},{48,64},{64,80},{80,96},{96,112},{112,128},... | collective-permute-start | bytes 9224 | tf_op jit(solution)/shard_map/ppermute | solution.py:26
  23.9 8.8 %copy-start.9 = (f32[1,2,128]{2,1,0:T(2,128)}, f32[1,2,128]{2,1,0:T(2,128)S(1)}, u32[]{:S(2)}) copy-start(f32[1,2,128]{2,1,0:T(2,128)S(1)} %reduce_window_sum.43) | copy-start | bytes 3076
  35.4 72.4 %copy-start.4 = (bf16[256,512]{1,0:T(8,128)(2,1)S(1)}, bf16[256,512]{1,0:T(8,128)(2,1)}, u32[]{:S(2)}) copy-start(bf16[256,512]{1,0:T(8,128)(2,1)} %param.33) | copy-start | bytes 786436
  38.2 49.7 %copy-start.7 = (f32[2,1,128,128]{3,2,1,0:T(8,128)}, f32[2,1,128,128]{3,2,1,0:T(8,128)S(1)}, u32[]{:S(2)}) copy-start(f32[2,1,128,128]{3,2,1,0:T(8,128)S(1)} %get-tuple-element.64) | copy-start | bytes 393220
  41.5 0.7 copy-start.6
  107.8 21.6 %copy-start.3 = (bf16[128,2048]{1,0:T(8,128)(2,1)S(1)}, bf16[128,2048]{1,0:T(8,128)(2,1)}, u32[]{:S(2)}) copy-start(bf16[128,2048]{1,0:T(8,128)(2,1)} %param.47) | copy-start | bytes 1572868
  108.3 20.3 %copy-start.8 = (bf16[256,128]{1,0:T(8,128)(2,1)S(1)}, bf16[256,128]{1,0:T(8,128)(2,1)}, u32[]{:S(2)}) copy-start(bf16[256,128]{1,0:T(8,128)(2,1)} %param.35) | copy-start | bytes 196612
  108.4 22.2 %copy-start.5 = (bf16[64,2048]{1,0:T(8,128)(2,1)S(1)}, bf16[64,2048]{1,0:T(8,128)(2,1)}, u32[]{:S(2)}) copy-start(bf16[64,2048]{1,0:T(8,128)(2,1)} %param.46) | copy-start | bytes 786436
  108.4 22.2 %copy-start.12 = (f32[64]{0:T(128)S(1)}, f32[64]{0:T(128)}, u32[]{:S(2)}) copy-start(f32[64]{0:T(128)} %param.44) | copy-start | bytes 772
  129.4 10.3 %copy-start.10 = (s32[256,3]{0,1:T(4,128)S(1)}, s32[256,3]{0,1:T(4,128)}, u32[]{:S(2)}) copy-start(s32[256,3]{0,1:T(4,128)} %param.49) | copy-start | bytes 9220
  132.1 36.1 %copy-start.2 = (bf16[256,2048]{1,0:T(8,128)(2,1)S(1)}, bf16[256,2048]{1,0:T(8,128)(2,1)}, u32[]{:S(2)}) copy-start(bf16[256,2048]{1,0:T(8,128)(2,1)} %param.29) | copy-start | bytes 3145732
  132.1 17.9 %all-to-all-start = ((bf16[16,16,2048]{2,1,0:T(8,128)(2,1)}), bf16[16,16,2048]{2,1,0:T(8,128)(2,1)S(1)}, u32[]{:S(2)}, u32[]{:S(2)}) async-start(bf16[16,16,2048]{2,1,0:T(8,128)(2,1)} %bitcast.113), calls=%async_computation | async-start | bytes 2097152 | tf_op jit(solution)/shard_map/all_to_all | solution.py:84
  151.3 16.9 %all-to-all-start.1 = ((bf16[16,16,2048]{2,1,0:T(8,128)(2,1)}), bf16[16,16,2048]{2,1,0:T(8,128)(2,1)S(1)}, u32[]{:S(2)}, u32[]{:S(2)}) async-start(bf16[16,16,2048]{2,1,0:T(8,128)(2,1)} %broadcast_in_dim.54), calls=%async_computation.1 | async-start | bytes 2097152 | tf_op jit(solution)/shard_map/all_to_all | solution.py:101
  168.6 1.3 copy-start.1
  205.8 54.3 %copy-start.13 = (bf16[1,2048,128]{2,1,0:T(8,128)(2,1)S(1)}, bf16[1,2048,128]{2,1,0:T(8,128)(2,1)}, u32[]{:S(2)}) copy-start(bf16[1,2048,128]{2,1,0:T(8,128)(2,1)} %param.51) | copy-start | bytes 1572868
  260.2 1.3 copy-start.14
  318.3 8.5 %copy-start.11 = (f32[256,3]{0,1:T(4,128)S(1)}, f32[256,3]{0,1:T(4,128)}, u32[]{:S(2)}) copy-start(f32[256,3]{0,1:T(4,128)} %param.50) | copy-start | bytes 9220
  321.9 27.6 %all-to-all-start.5 = ((bf16[32,32,128]{2,1,0:T(8,128)(2,1)}), bf16[32,32,128]{2,1,0:T(8,128)(2,1)S(1)}, u32[]{:S(2)}, u32[]{:S(2)}) async-start(bf16[32,32,128]{2,1,0:T(8,128)(2,1)} %reduce_sum.97), calls=%async_computation.5 | async-start | bytes 524288 | tf_op jit(solution)/shard_map/all_to_all | solution.py:368
where the time goes:
time: 359 us; the launch traced here: 354 us
  blocking collectives  178 us (50%)
  local copies, waits for them, and re-layouts  42.4 us (12%)
  waiting for transfers between devices  32.3 us (9%)
  starting transfers between devices  30.7 us (9%)
  between operations  30.2 us (8%)
  other arithmetic  25.9 us (7%)
  matrix products  13.5 us (4%)
    all_to_all x1, blocking collectives, from_everyone(): return lax.all_to_all(copies, axis, split_axis=0, concat_axis=0, tiled=True)  54.3 us
    all_to_all x1, blocking collectives, sent_and_summed(): parts = lax.all_to_all(split_up(x, dim, length), axis, 0, 0, tiled=True)  53.2 us
    all_gather x2, blocking collectives, all_in_one(): both, at, found = (lax.all_gather(jnp.concatenate(lines), axis), 0, {})  39.2 us
    all_to_all x1, blocking collectives, local(): lax.all_to_all(outgoing.reshape(experts, capacity, column_width), SP, spl...  31.6 us
    all_to_all x1, waiting for transfers between devices, local(): lax.all_to_all(summed.astype(jnp.bfloat16), SP, split_axis=0, concat_axis...  22.5 us
    ppermute x4, starting transfers between devices, passed_along(): return lax.ppermute(block, axis, route)  11.6 us
    all_to_all x1, waiting for transfers between devices, sent_and_summed(): parts = lax.all_to_all(split_up(x, dim, length), axis, 0, 0, tiled=True)  7.71 us
    all_to_all x1, starting transfers between devices, sent_and_summed(): parts = lax.all_to_all(split_up(x, dim, length), axis, 0, 0, tiled=True)  7.55 us
  transfers between devices with their start and end apart: 7, of which 3 were waited for; matrix products, arithmetic and copies ran while one was open for 13% of the time, Pallas kernels for 0%

commit v1 on v0

--- a/solution.py
+++ b/solution.py
@@ -3,7 +3,8 @@
 import jax
 import jax.numpy as jnp
 from jax import lax
-from jax.sharding import Mesh
+from jax.experimental import pallas as pl
+from jax.experimental.pallas import tpu as pltpu
 from jax.sharding import PartitionSpec as P
 
 HEADS = 16
@@ -11,7 +12,7 @@
 WIDE_HEAD_DIM = 128
 GROUPS = 4
 BLOCK = 128
-SP = ("sp_0", "sp_1")
+SP = "sp"
 
 
 NORM_EPS = 1e-06
@@ -52,7 +53,7 @@
 def entering_2(x, axes, combine, identity):
     before = start = filled_with(x, identity)
     running = x
-    for axis in reversed(axes):
+    for axis in (axes,):
         length, mine = (lax.axis_size(axis), lax.axis_index(axis))
         pieces = all_in_one(
             jax.tree.map(
@@ -208,6 +209,454 @@
         jnp.exp(later[0])[:, None, None] * earlier[2] + later[2],
         jnp.exp(later[1])[:, None, None] * earlier[3] + later[3],
     )
+
+
+MESH = pl.DeviceIdType.MESH
+CORES = 2
+SIDE = 4
+
+
+def remote(src, dst, send_sem, recv_sem, device):
+    return pltpu.make_async_remote_copy(
+        src_ref=src,
+        dst_ref=dst,
+        send_sem=send_sem,
+        recv_sem=recv_sem,
+        device_id=device,
+        device_id_type=MESH,
+    )
+
+
+class Place:
+    def __init__(self, chips):
+        self.chips = chips
+        self.sp = lax.axis_index("sp")
+        self.tp = lax.axis_index("tp")
+        self.z, self.core = self.sp // CORES, self.sp % CORES
+        self.at = {"y": self.tp // SIDE, "x": self.tp % SIDE}
+
+    def plane(self, axis, step):
+        moved = (self.at[axis] + step + SIDE) % SIDE
+        if axis == "x":
+            return (self.sp, self.at["y"] * SIDE + moved)
+        return (self.sp, moved * SIDE + self.at["x"])
+
+    def index(self, axis, step):
+        return (self.at[axis] + step + SIDE) % SIDE
+
+    def along(self, step, core):
+        return (((self.z + step + self.chips) % self.chips) * CORES + core, self.tp)
+
+
+def chip_order(chips):
+    if chips == 16:
+        return [1, 15, 3, 13, 5, 11, 7, 9, 8, 6, 10, 4, 12, 2, 14, 0]
+    return [d % chips for d in range(1, chips + 1)]
+
+
+def greet(place):
+    barrier = pltpu.get_barrier_semaphore()
+    count = 0
+    for axis in ("x", "y"):
+        for step in (1, SIDE - 1):
+            pl.semaphore_signal(barrier, inc=1, device_id=place.plane(axis, step), device_id_type=MESH)
+            count += 1
+    for step in range(place.chips):
+        if step:
+            pl.semaphore_signal(
+                barrier, inc=1, device_id=place.along(step, place.core), device_id_type=MESH
+            )
+            count += 1
+        pl.semaphore_signal(
+            barrier, inc=1, device_id=place.along(step, 1 - place.core), device_id_type=MESH
+        )
+        count += 1
+    return barrier, count
+
+
+def chunk_of(ref, axis, index):
+    return ref.at[index] if axis == "y" else ref.at[:, index]
+
+
+class Summer:
+    def __init__(self, place, first, blocks, relay, sums, half, last, sent, got):
+        self.place, self.first, self.second = place, first, "y" if first == "x" else "x"
+        self.blocks, self.relay, self.sums = blocks, relay, sums
+        self.half, self.last, self.sent, self.got = half, last, sent, got
+        self.started = []
+        rows = blocks.shape[2]
+        self.low, self.high = pl.ds(0, rows // 2), pl.ds(rows // 2, rows // 2)
+
+    def send(self, src, dst, axis, step, number):
+        copy = remote(
+            src, dst, self.sent.at[number], self.got.at[number], self.place.plane(axis, step)
+        )
+        copy.start()
+        self.started.append(copy)
+
+    def open(self):
+        far = chunk_of(self.blocks, self.first, self.place.index(self.first, 2))
+        self.send(far.at[:, self.low], self.relay.at[0], self.first, 1, 0)
+        self.send(far.at[:, self.high], self.relay.at[1], self.first, SIDE - 1, 1)
+
+    def pass_on(self):
+        for side, step in ((0, 1), (1, SIDE - 1)):
+            part = self.low if side == 0 else self.high
+            self.started[side].wait_recv()
+            near = chunk_of(self.blocks, self.first, self.place.index(self.first, step))
+            piece = near.at[:, part]
+            piece[...] = (
+                piece[...].astype(jnp.float32) + self.relay[side].astype(jnp.float32)
+            ).astype(jnp.bfloat16)
+            self.send(near, self.sums.at[side], self.first, step, 2 + side)
+
+    def turn(self):
+        self.started[2].wait_recv()
+        self.started[3].wait_recv()
+        own = chunk_of(self.blocks, self.first, self.place.at[self.first])
+        own[...] = (
+            own[...].astype(jnp.float32)
+            + self.sums[0].astype(jnp.float32)
+            + self.sums[1].astype(jnp.float32)
+        ).astype(jnp.bfloat16)
+        far = own.at[self.place.index(self.second, 2)]
+        self.send(far.at[self.low], self.half.at[0], self.second, 1, 4)
+        self.send(far.at[self.high], self.half.at[1], self.second, SIDE - 1, 5)
+
+    def pass_again(self):
+        own = chunk_of(self.blocks, self.first, self.place.at[self.first])
+        for side, step in ((0, 1), (1, SIDE - 1)):
+            part = self.low if side == 0 else self.high
+            self.started[4 + side].wait_recv()
+            near = own.at[self.place.index(self.second, step)]
+            piece = near.at[part]
+            piece[...] = (
+                piece[...].astype(jnp.float32) + self.half[side].astype(jnp.float32)
+            ).astype(jnp.bfloat16)
+            self.send(near, self.last.at[side], self.second, step, 6 + side)
+
+    def close(self):
+        self.started[6].wait_recv()
+        self.started[7].wait_recv()
+        own = chunk_of(self.blocks, self.first, self.place.at[self.first])
+        mine = own.at[self.place.at[self.second]]
+        return (
+            mine[...].astype(jnp.float32)
+            + self.last[0].astype(jnp.float32)
+            + self.last[1].astype(jnp.float32)
+        )
+
+
+class Spreader:
+    def __init__(self, place, first, blocks, sent, got):
+        self.place, self.first, self.second = place, first, "y" if first == "x" else "x"
+        self.blocks, self.sent, self.got = blocks, sent, got
+        self.started = []
+        rows = blocks.shape[2]
+        self.low, self.high = pl.ds(0, rows // 2), pl.ds(rows // 2, rows // 2)
+
+    def send(self, ref, axis, step, number):
+        copy = remote(
+            ref, ref, self.sent.at[number], self.got.at[number], self.place.plane(axis, step)
+        )
+        copy.start()
+        self.started.append(copy)
+
+    def block(self, step):
+        line = chunk_of(self.blocks, self.second, self.place.at[self.second])
+        return line.at[self.place.index(self.first, step)]
+
+    def line(self, step):
+        return chunk_of(self.blocks, self.second, self.place.index(self.second, step))
+
+    def open(self):
+        self.send(self.block(0), self.first, 1, 0)
+        self.send(self.block(0), self.first, SIDE - 1, 1)
+
+    def pass_on(self):
+        self.started[0].wait_recv()
+        self.send(self.block(SIDE - 1).at[self.low], self.first, 1, 2)
+        self.started[1].wait_recv()
+        self.send(self.block(1).at[self.high], self.first, SIDE - 1, 3)
+
+    def turn(self):
+        self.started[2].wait_recv()
+        self.started[3].wait_recv()
+        self.send(self.line(0), self.second, 1, 4)
+        self.send(self.line(0), self.second, SIDE - 1, 5)
+
+    def pass_again(self):
+        self.started[4].wait_recv()
+        self.send(self.line(SIDE - 1).at[:, self.low], self.second, 1, 6)
+        self.started[5].wait_recv()
+        self.send(self.line(1).at[:, self.high], self.second, SIDE - 1, 7)
+
+    def close(self):
+        self.started[6].wait_recv()
+        self.started[7].wait_recv()
+
+
+def iota(shape, dim):
+    return lax.broadcasted_iota(jnp.int32, shape, dim)
+
+
+def ones_where(mask):
+    return jnp.where(mask, 1.0, 0.0).astype(jnp.bfloat16)
+
+
+def dot(a, b):
+    return jnp.dot(a, b, preferred_element_type=jnp.float32)
+
+
+def in_two(x):
+    high = x.astype(jnp.bfloat16)
+    return high, (x - high.astype(jnp.float32)).astype(jnp.bfloat16)
+
+
+def routing_tables(experts, cap, routes, routes_turned, weights, choice, share):
+    tokens, picks = routes.shape
+    slots = experts * cap
+    shift = cap.bit_length() - 1
+    named = routes[...]
+    turned = routes_turned[...]
+    amount = weights[...]
+    lines = iota((experts, tokens), 0)
+    there = turned[0:1, :] == lines
+    for k in range(1, picks):
+        there = there | (turned[k : k + 1, :] == lines)
+    before = ones_where(iota((tokens, tokens), 0) < iota((tokens, tokens), 1))
+    rank = jnp.where(there, dot(ones_where(there), before), -1.0).astype(jnp.bfloat16)
+    spread = ones_where((iota((slots, experts), 0) >> shift) == iota((slots, experts), 1))
+    wide = dot(spread, rank)
+    number = (iota((slots, tokens), 0) & (cap - 1)).astype(jnp.float32)
+    choice[...] = ones_where(wide == number)
+
+    columns = iota((tokens, experts), 1)
+    hit = named[:, 0:1] == columns
+    weight = jnp.where(hit, amount[:, 0:1], 0.0)
+    for k in range(1, picks):
+        now = named[:, k : k + 1] == columns
+        hit = hit | now
+        weight = weight + jnp.where(now, amount[:, k : k + 1], 0.0)
+    after = ones_where(iota((tokens, tokens), 1) < iota((tokens, tokens), 0))
+    rank = jnp.where(hit, dot(after, ones_where(hit)), -1.0).astype(jnp.bfloat16)
+    spread = ones_where(iota((experts, slots), 0) == (iota((experts, slots), 1) >> shift))
+    wide = dot(rank, spread)
+    number = (iota((tokens, slots), 1) & (cap - 1)).astype(jnp.float32)
+    mine = wide == number
+    for part, piece in enumerate(in_two(weight)):
+        share[part] = jnp.where(mine, dot(piece, spread), 0.0).astype(jnp.bfloat16)
+
+
+def expert_kernel(
+    chips,
+    cap,
+    unit_chips,
+    normed,
+    state,
+    routes,
+    routes_turned,
+    weights,
+    gate_hbm,
+    up_hbm,
+    down_hbm,
+    out,
+    choice,
+    share,
+    outgoing,
+    tokens,
+    gate_up,
+    down,
+    partial,
+    relay,
+    sums,
+    half,
+    last,
+    result,
+    back,
+    load_sem,
+    out_sent,
+    out_got,
+    spread_sent,
+    spread_got,
+    sum_sent,
+    sum_got,
+    back_sent,
+    back_got,
+):
+    place = Place(chips)
+    experts = chips * CORES
+    barrier, count = greet(place)
+    loads = [
+        pltpu.make_async_copy(gate_hbm, gate_up.at[:, pl.ds(0, gate_hbm.shape[1])], load_sem.at[0]),
+        pltpu.make_async_copy(
+            up_hbm, gate_up.at[:, pl.ds(gate_hbm.shape[1], gate_hbm.shape[1])], load_sem.at[1]
+        ),
+        pltpu.make_async_copy(down_hbm, down, load_sem.at[2]),
+    ]
+    for load in loads:
+        load.start()
+    routing_tables(experts, cap, routes, routes_turned, weights, choice, share)
+    outgoing[...] = dot(choice[...], normed[...]).astype(jnp.bfloat16)
+    pl.semaphore_wait(barrier, count)
+
+    order = chip_order(chips)
+    spot = {d: k for k, d in enumerate(order)}
+    y, x = place.at["y"], place.at["x"]
+
+    def slot_rows(number):
+        return pl.ds(pl.multiple_of(number * cap, cap), cap)
+
+    dispatch = {}
+    for d in order:
+        for other in (0, 1):
+            core = place.core if other == 0 else 1 - place.core
+            device = place.along((chips - d) % chips, core)
+            rows = slot_rows(device[0])
+            to = slot_rows(spot[d] * CORES + place.core)
+            if d == 0 and other == 0:
+                tokens[y, x, to, :] = outgoing[rows, :]
+                continue
+            number = spot[d] * CORES + other
+            copy = remote(
+                outgoing.at[rows],
+                tokens.at[y, x, to],
+                out_sent.at[number],
+                out_got.at[number],
+                device,
+            )
+            copy.start()
+            dispatch[(d, other)] = copy
+
+    unit = unit_chips * CORES * cap
+    units = chips // unit_chips
+    width = gate_hbm.shape[1]
+    returns = {}
+
+    def steps(u):
+        first = "x" if u % 2 == 0 else "y"
+        rows = pl.ds(u * unit, unit)
+        spread = Spreader(
+            place, first, tokens.at[:, :, rows], spread_sent.at[u], spread_got.at[u]
+        )
+        total = Summer(
+            place, first, partial.at[u], relay.at[u], sums.at[u], half.at[u], last.at[u],
+            sum_sent.at[u], sum_got.at[u],
+        )
+
+        def arrive():
+            for d in order[u * unit_chips : (u + 1) * unit_chips]:
+                for other in (0, 1):
+                    if (d, other) in dispatch:
+                        dispatch[(d, other)].wait_recv()
+            spread.open()
+
+        def compute():
+            spread.close()
+            if u == 0:
+                for load in loads:
+                    load.wait()
+            lines = jnp.concatenate(
+                [tokens[i, j, rows, :] for i in range(SIDE) for j in range(SIDE)], axis=1
+            )
+            both = dot(lines, gate_up[...])
+            gate = jnp.minimum(both[:, :width], CLAMP_LIMIT)
+            up = jnp.clip(both[:, width:], -CLAMP_LIMIT, CLAMP_LIMIT)
+            act = ((up + 1.0) * gate * jax.nn.sigmoid(SIGMOID_SCALE * gate)).astype(jnp.bfloat16)
+            for i in range(SIDE):
+                wide = dot(act, down[:, i * SIDE * width : (i + 1) * SIDE * width])
+                for j in range(SIDE):
+                    partial[u, i, j] = wide[:, j * width : (j + 1) * width].astype(jnp.bfloat16)
+            total.open()
+
+        def close():
+            result[u] = total.close().astype(jnp.bfloat16)
+            for k, d in enumerate(order[u * unit_chips : (u + 1) * unit_chips]):
+                for other in (0, 1):
+                    core = place.core if other == 0 else 1 - place.core
+                    piece = slot_rows(k * CORES + core)
+                    to = slot_rows(place.sp)
+                    if d == 0 and other == 0:
+                        back[to, :] = result[u, piece, :]
+                        continue
+                    number = spot[d] * CORES + other
+                    copy = remote(
+                        result.at[u, piece],
+                        back.at[to],
+                        back_sent.at[number],
+                        back_got.at[number],
+                        place.along(d, core),
+                    )
+                    copy.start()
+                    returns[(d, other)] = copy
+
+        plan = [
+            arrive, spread.pass_on, spread.turn, spread.pass_again, compute,
+            total.pass_on, total.turn, total.pass_again, close,
+        ]
+        return plan, spread, total
+
+    plans = [steps(u) for u in range(units)]
+    depth = len(plans[0][0])
+    for tick in range(units + depth - 1):
+        for u in range(units):
+            if 0 <= tick - u < depth:
+                plans[u][0][tick - u]()
+    for copy in returns.values():
+        copy.wait_recv()
+    combined = state[...] + dot(share[0], back[...]) + dot(share[1], back[...])
+    out[...] = combined.astype(jnp.bfloat16)
+    for copy in list(dispatch.values()) + list(returns.values()):
+        copy.wait_send()
+    for _, spread, total in plans:
+        for copy in spread.started + total.started:
+            copy.wait_send()
+
+
+def expert_layer(normed, state, routes, weights, gate, up, down, chips, unit_chips):
+    length, width = normed.shape
+    experts = chips * CORES
+    picks = routes.shape[1]
+    cap = 4 * length * picks // (3 * experts)
+    features = gate.shape[0]
+    unit = unit_chips * CORES * cap
+    units = chips // unit_chips
+    slots = experts * cap
+    vmem, any_ = pl.BlockSpec(memory_space=pltpu.VMEM), pl.BlockSpec(memory_space=pl.ANY)
+    bf16 = jnp.bfloat16
+    return pl.pallas_call(
+        functools.partial(expert_kernel, chips, cap, unit_chips),
+        out_shape=jax.ShapeDtypeStruct((length, width), bf16),
+        in_specs=[vmem] * 5 + [any_] * 3,
+        out_specs=vmem,
+        scratch_shapes=[
+            pltpu.VMEM((slots, length), bf16),
+            pltpu.VMEM((2, length, slots), bf16),
+            pltpu.VMEM((slots, width), bf16),
+            pltpu.VMEM((SIDE, SIDE, slots, width), bf16),
+            pltpu.VMEM((features, 2 * gate.shape[1]), bf16),
+            pltpu.VMEM(down.shape, bf16),
+            pltpu.VMEM((units, SIDE, SIDE, unit, width), bf16),
+            pltpu.VMEM((units, 2, SIDE, unit // 2, width), bf16),
+            pltpu.VMEM((units, 2, SIDE, unit, width), bf16),
+            pltpu.VMEM((units, 2, unit // 2, width), bf16),
+            pltpu.VMEM((units, 2, unit, width), bf16),
+            pltpu.VMEM((units, unit, width), bf16),
+            pltpu.VMEM((slots, width), bf16),
+            pltpu.SemaphoreType.DMA((3,)),
+            pltpu.SemaphoreType.DMA((experts,)),
+            pltpu.SemaphoreType.DMA((experts,)),
+            pltpu.SemaphoreType.DMA((units, 8)),
+            pltpu.SemaphoreType.DMA((units, 8)),
+            pltpu.SemaphoreType.DMA((units, 8)),
+            pltpu.SemaphoreType.DMA((units, 8)),
+            pltpu.SemaphoreType.DMA((experts,)),
+            pltpu.SemaphoreType.DMA((experts,)),
+        ],
+        compiler_params=pltpu.CompilerParams(
+            collective_id=1, has_side_effects=True, vmem_limit_bytes=56 * 1024 * 1024
+        ),
+    )(normed, state, routes, routes.T, weights, gate, up, down)
 
 
 def local(
@@ -320,65 +769,27 @@
         * lax.rsqrt(jnp.mean(hidden_state * hidden_state, axis=-1, keepdims=True) + NORM_EPS)
         * feedforward_norm_gain
     ).astype(jnp.bfloat16)
-    experts = lax.axis_size(SP)
-    picks = routes.shape[1]
-    capacity = 4 * length * picks // (3 * experts)
     column_width = normed.shape[1] // lax.axis_size("tp")
     tp_index = lax.axis_index("tp")
-    flat_routes = routes.reshape(-1)
-    member_hits = (flat_routes[:, None] == jnp.arange(experts, dtype=jnp.int32)[None, :]).astype(
-        jnp.int32
-    )
-    ranks = jnp.sum((jnp.cumsum(member_hits, axis=0) - member_hits) * member_hits, axis=1)
-    slot_ids = flat_routes * capacity + ranks
-    source_rows = (
-        jnp.zeros((experts * capacity,), jnp.int32)
-        .at[slot_ids]
-        .set(jnp.arange(length * picks, dtype=jnp.int32) // picks)
-    )
-    occupied = jnp.zeros((experts * capacity,), jnp.int32).at[slot_ids].set(1)
-    gate_weight = expert_gate_matrix[0]
-    up_weight = expert_up_matrix[0]
-    down_weight = expert_down_matrix[0]
     own_columns = lax.dynamic_slice_in_dim(normed, tp_index * column_width, column_width, 1)
-    outgoing = jnp.where(
-        occupied[:, None] > 0, own_columns[source_rows], jnp.zeros((), jnp.bfloat16)
-    )
-    arrived = lax.all_to_all(
-        outgoing.reshape(experts, capacity, column_width),
-        SP,
-        split_axis=0,
-        concat_axis=0,
-        tiled=True,
-    )
-    slot_parts = arrived.reshape(experts * capacity, column_width)
-    piece = collect(slot_parts, "tp", 1)
-    gate_pre = jnp.dot(piece, gate_weight, preferred_element_type=jnp.float32)
-    up_pre = jnp.dot(piece, up_weight, preferred_element_type=jnp.float32)
-    clamped = jnp.minimum(gate_pre, CLAMP_LIMIT)
-    act = (
-        (jnp.clip(up_pre, -CLAMP_LIMIT, CLAMP_LIMIT) + 1.0)
-        * clamped
-        * jax.nn.sigmoid(SIGMOID_SCALE * clamped)
-    ).astype(jnp.bfloat16)
-    partial_out = jnp.dot(act, down_weight, preferred_element_type=jnp.float32)
-    summed = sent_and_summed(
-        partial_out.reshape(experts, capacity, -1).astype(jnp.bfloat16), "tp", 2
-    )
-    returned = lax.all_to_all(
-        summed.astype(jnp.bfloat16), SP, split_axis=0, concat_axis=0, tiled=True
-    )
-    token_rows = returned.reshape(experts * capacity, -1)[slot_ids].reshape(length, picks, -1)
-    combined = jnp.sum(token_rows.astype(jnp.float32) * routing_weight_values[..., None], axis=1)
     own_state = lax.dynamic_slice_in_dim(hidden_state, tp_index * column_width, column_width, 1)
-    return (own_state + combined).astype(jnp.bfloat16)
+    return expert_layer(
+        own_columns,
+        own_state,
+        routes,
+        routing_weight_values,
+        expert_gate_matrix[0],
+        expert_up_matrix[0],
+        expert_down_matrix[0],
+        lax.axis_size(SP) // CORES,
+        2,
+    )
 
 
 def solution(mesh):
-    finer = Mesh(mesh.devices.reshape(16, 2, mesh.shape["tp"]), ("sp_0", "sp_1", "tp"))
     return jax.shard_map(
         local,
-        mesh=finer,
+        mesh=mesh,
         in_specs=(
             P(SP, None),
             P(SP, "tp"),

time: 359 us -> 340 us (0.947)
  blocking collectives: 178 us -> 22 us
  Pallas kernels: 0 us -> 93.1 us
  waiting for transfers between devices: 32.3 us -> 79.6 us
  between operations: 30.2 us -> 58 us
  starting transfers between devices: 30.7 us -> 17.8 us
  matrix products: 13.5 us -> 5.68 us
  other arithmetic: 25.9 us -> 19.8 us
    pallas_call x0 -> x1, Pallas kernels: none -> 93.1 us  [expert_layer(): pl.pallas_call(functools.partial(expert_kernel, chips, cap, unit_chips),...]
    all_to_all x2 -> x0, blocking collectives: 86 us -> none  [the longest x1 54.3 us: from_everyone(): return lax.all_to_all(copies, axis, split_axis=0, concat_axis=0, tiled=True)]
    all_gather x0 -> x1, waiting for transfers between devices: none -> 68.1 us  [all_in_one(): both, at, found = (lax.all_gather(jnp.concatenate(lines), axis), 0, {})]
    all_gather x2 -> x0, blocking collectives: 39.2 us -> none  [all_in_one(): both, at, found = (lax.all_gather(jnp.concatenate(lines), axis), 0, {})]
    all_to_all x1, blocking collectives: 53.2 us -> 22 us  [sent_and_summed(): parts = lax.all_to_all(split_up(x, dim, length), axis, 0, 0, tiled=True)]
    all_to_all x2 -> x0, waiting for transfers between devices: 30.2 us -> none  [the longest x1 22.5 us: local(): lax.all_to_all(summed.astype(jnp.bfloat16), SP, split_axis=0, concat_axis...]
    convert_element_type x8 -> x24, local copies, waits for them, and re-layouts: 5.55 us -> 20.6 us  [entering_2(): part[k].astype(own.dtype)]
    all_to_all x2 -> x0, starting transfers between devices: 12.5 us -> none  [the longest x1 7.55 us: sent_and_summed(): parts = lax.all_to_all(split_up(x, dim, length), axis, 0, 0, tiled=True)]
  transfers between devices with their start and end apart: 7 -> 6, of which waited for: 3 -> 2; matrix products, arithmetic and copies ran while one was open for 13% -> 5% of each run, Pallas kernels for 0% -> 0%
where the time goes in v1:
time: 340 us; the launch traced here: 337 us
  Pallas kernels  93.1 us (27%)
  waiting for transfers between devices  79.6 us (23%)
  between operations  58 us (17%)
  local copies, waits for them, and re-layouts  40.4 us (12%)
  blocking collectives  22 us (6%)
  other arithmetic  19.8 us (6%)
  starting transfers between devices  17.8 us (5%)
  matrix products  5.68 us (2%)
    pallas_call x1, Pallas kernels, expert_layer(): pl.pallas_call(functools.partial(expert_kernel, chips, cap, unit_chips),...  93.1 us
    all_gather x1, waiting for transfers between devices, all_in_one(): both, at, found = (lax.all_gather(jnp.concatenate(lines), axis), 0, {})  68.1 us
    all_to_all x1, blocking collectives, sent_and_summed(): parts = lax.all_to_all(split_up(x, dim, length), axis, 0, 0, tiled=True)  22 us
    convert_element_type x24, local copies, waits for them, and re-layouts, entering_2(): part[k].astype(own.dtype)  20.6 us
    ppermute x4, starting transfers between devices, passed_along(): return lax.ppermute(block, axis, route)  11.7 us
    all_to_all x1, waiting for transfers between devices, from_everyone(): return lax.all_to_all(copies, axis, split_axis=0, concat_axis=0, tiled=True)  11.5 us
  transfers between devices with their start and end apart: 6, of which 2 were waited for; matrix products, arithmetic and copies ran while one was open for 5% of the time, Pallas kernels for 0%

profile of v1, /device:TPU:6, one launch (start us, length us, event | category | flops | bytes accessed | tf_op | source)
XLA Modules:
  0.0 336.5 jit_solution(10477664133695011870)
XLA Ops:
  7.3 1.7 collective-permute-start.3
  9.7 4.1 %collective-permute-start.1 = (bf16[3,512]{1,0:T(4,128)(2,1)S(1)}, bf16[3,512]{1,0:T(4,128)(2,1)S(1)}, u32[]{:S(2)}, u32[]{:S(2)}) collective-permute-start(bf16[3,512]{1,0:T(4,128)(2,1)S(1)} %slice.736), channel_id=1, source_target_pairs={{0,16},{16,32},{32,48},{48,64},{64,80},{80,96},{96,112},{112,128},... | collective-permute-start | bytes 9224 | tf_op jit(solution)/shard_map/ppermute | solution.py:27
  13.8 0.8 slice.748
  14.6 1.9 collective-permute-start.2
  16.6 1.3 fusion.87
  22.6 0.8 slice_bitcast_fusion.7
  23.4 0.8 slice_bitcast_fusion.3
  24.4 0.9 fusion.84
  25.2 1.2 pad_bitcast_fusion
  26.5 0.8 maximum_convert_fusion.3
  27.5 0.9 maximum_convert_fusion.2
  28.5 1.0 maximum_convert_fusion.1
  31.0 2.6 while.27
  34.0 2.8 while.26
  37.6 3.9 %collective-permute-start = (bf16[3,512]{1,0:T(4,128)(2,1)S(1)}, bf16[3,512]{1,0:T(4,128)(2,1)S(1)}, u32[]{:S(2)}, u32[]{:S(2)}) collective-permute-start(bf16[3,512]{1,0:T(4,128)(2,1)S(1)} %slice.727), channel_id=1, source_target_pairs={{0,16},{16,32},{32,48},{48,64},{64,80},{80,96},{96,112},{112,128},... | collective-permute-start | bytes 9224 | tf_op jit(solution)/shard_map/ppermute | solution.py:27
  45.1 68.1 %all-gather.4.cloned.1.call-done = bf16[32,194,128]{2,1,0:T(8,128)(2,1)} async-done(((bf16[1,194,128]{2,1,0:T(8,128)(2,1)}), bf16[32,194,128]{2,1,0:T(8,128)(2,1)}) %all-gather.4.cloned.1.call-update) | async-done | bytes 1589264 | tf_op jit(solution)/shard_map/all_gather | solution.py:44
  113.2 0.9 fusion.79
  159.4 0.9 select_select_fusion.1
  160.3 0.9 multiply_add_fusion
  161.3 0.8 slice_convert_fusion.4
  162.2 1.7 slice_convert_fusion.23
  164.5 0.9 reshape.1701
  165.4 1.5 reshape.1700
  166.9 1.5 reshape.1699
  168.4 1.5 reshape.1698
  169.8 1.5 reshape.1697
  171.3 1.4 reshape.1696
  172.7 1.5 reshape.1695
  174.2 1.5 reshape.1694
  175.7 1.5 reshape.1693
  177.1 1.5 reshape.1692
  178.6 1.5 reshape.1691
  180.0 1.5 reshape.1690
  181.5 1.5 reshape.1689
  182.9 1.4 reshape.1688
  184.4 1.5 select_select_fusion
  185.9 1.4 fusion.1
  188.8 0.8 multiply_reduce_fusion.1
  190.6 22.0 %all_to_all.10 = bf16[16,16,2048]{2,1,0:T(8,128)(2,1)S(1)} all-to-all(bf16[16,16,2048]{2,1,0:T(8,128)(2,1)S(1)} %bitcast.231), channel_id=1, replica_groups=mesh['sp'=32,'tp'=16] {'tp'}, dimensions={0} | all-to-all | bytes 2097152 | tf_op jit(solution)/shard_map/all_to_all | solution.py:85
  212.7 1.1 broadcast_in_dim.38
  213.8 6.2 %all-to-all-start.1 = ((bf16[16,16,2048]{2,1,0:T(8,128)(2,1)}), bf16[16,16,2048]{2,1,0:T(8,128)(2,1)S(1)}, u32[]{:S(2)}, u32[]{:S(2)}) async-start(bf16[16,16,2048]{2,1,0:T(8,128)(2,1)} %broadcast_in_dim.38), calls=%async_computation.1 | async-start | bytes 2097152 | tf_op jit(solution)/shard_map/all_to_all | solution.py:102
  220.0 0.8 copy.82.weights
  220.8 0.8 copy.81.routes
  221.6 0.8 dynamic-slice
  222.4 11.5 %all-to-all-done.1 = bf16[16,16,2048]{2,1,0:T(8,128)(2,1)S(1)} async-done(((bf16[16,16,2048]{2,1,0:T(8,128)(2,1)}), bf16[16,16,2048]{2,1,0:T(8,128)(2,1)S(1)}, u32[]{:S(2)}, u32[]{:S(2)}) %all-to-all-start.1) | async-done | bytes 1048608 | tf_op jit(solution)/shard_map/all_to_all | solution.py:102
  234.3 0.7 multiply_convert_fusion
  235.0 93.1 %shard_map.235 = bf16[256,128]{1,0:T(8,128)(2,1)} custom-call(bf16[256,128]{1,0:T(8,128)(2,1)} %get-tuple-element.175.normed, f32[256,128]{1,0:T(8,128)} %get-tuple-element.176.state, s32[256,3]{1,0:T(8,128)} %copy.81.routes, s32[3,256]{1,0:T(4,128)} %bitcast.249, f32[256,3]{1,0:T(8,128)} %copy.82.weights, bf16[2048,128]{1,0:T(8,128)(2,1)} %bitcast.240, ...), custom_call_target="tpu_custom_call" | custom-call | tf_op jit(solution)/shard_map/pallas_call | solution.py:627
  328.2 1.5 copy.137
  (123 shorter events, 23.0 us)
Async XLA Ops:
  6.5 183.0 %copy-start = (bf16[128,2048]{1,0:T(8,128)(2,1)S(1)}, bf16[128,2048]{1,0:T(8,128)(2,1)}, u32[]{:S(2)}) copy-start(bf16[128,2048]{1,0:T(8,128)(2,1)} %param.47) | copy-start | bytes 1572868
  6.5 106.6 %all-gather.4.cloned.1.call-start = ((), (), s32[]{:S(2)}) async-start(), calls=%async_computation.2 | async-start | bytes 1689600 | tf_op jit(solution)/shard_map/all_gather | solution.py:44
  7.3 20.2 %collective-permute-start.3 = (bf16[3,128]{1,0:T(4,128)(2,1)S(1)}, bf16[3,128]{1,0:T(4,128)(2,1)S(1)}, u32[]{:S(2)}, u32[]{:S(2)}) collective-permute-start(bf16[3,128]{1,0:T(4,128)(2,1)S(1)} %slice.762), channel_id=1, source_target_pairs={{0,16},{16,32},{32,48},{48,64},{64,80},{80,96},{96,112},{112,128},... | collective-permute-start | bytes 2312 | tf_op jit(solution)/shard_map/ppermute | solution.py:27
  9.7 18.8 %collective-permute-start.1 = (bf16[3,512]{1,0:T(4,128)(2,1)S(1)}, bf16[3,512]{1,0:T(4,128)(2,1)S(1)}, u32[]{:S(2)}, u32[]{:S(2)}) collective-permute-start(bf16[3,512]{1,0:T(4,128)(2,1)S(1)} %slice.736), channel_id=1, source_target_pairs={{0,16},{16,32},{32,48},{48,64},{64,80},{80,96},{96,112},{112,128},... | collective-permute-start | bytes 9224 | tf_op jit(solution)/shard_map/ppermute | solution.py:27
  14.6 11.8 %collective-permute-start.2 = (bf16[3,64]{0,1:T(8,128)(2,1)S(1)}, bf16[3,64]{0,1:T(8,128)(2,1)S(1)}, u32[]{:S(2)}, u32[]{:S(2)}) collective-permute-start(bf16[3,64]{0,1:T(8,128)(2,1)S(1)} %slice.748), channel_id=1, source_target_pairs={{0,16},{16,32},{32,48},{48,64},{64,80},{80,96},{96,112},{112,128},... | collective-permute-start | bytes 1160 | tf_op jit(solution)/shard_map/ppermute | solution.py:27
  33.6 9.2 %copy-start.6 = (f32[2,1,128,128]{3,2,1,0:T(8,128)}, f32[2,1,128,128]{3,2,1,0:T(8,128)S(1)}, u32[]{:S(2)}) copy-start(f32[2,1,128,128]{3,2,1,0:T(8,128)S(1)} %get-tuple-element.64) | copy-start | bytes 393220
  33.6 4.0 %copy-start.3 = (bf16[256,512]{1,0:T(8,128)(2,1)S(1)}, bf16[256,512]{1,0:T(8,128)(2,1)}, u32[]{:S(2)}) copy-start(bf16[256,512]{1,0:T(8,128)(2,1)} %param.33) | copy-start | bytes 786436
  33.6 8.3 %copy-start.13 = (f32[2,1]{0,1:T(1,128)S(1)}, f32[2,1]{0,1:T(1,128)}, u32[]{:S(2)}) copy-start(f32[2,1]{0,1:T(1,128)} %param.39) | copy-start | bytes 28
  33.6 9.0 %copy-start.11 = (f32[4,512]{1,0:T(4,128)S(1)}, f32[4,512]{1,0:T(4,128)}, u32[]{:S(2)}) copy-start(f32[4,512]{1,0:T(4,128)} %param.43) | copy-start | bytes 24580
  36.8 5.1 %copy-start.5 = (f32[2,1,128,64]{3,2,1,0:T(8,128)}, f32[2,1,128,64]{3,2,1,0:T(8,128)S(1)}, u32[]{:S(2)}) copy-start(f32[2,1,128,64]{3,2,1,0:T(8,128)S(1)} %get-tuple-element.61) | copy-start | bytes 196612
  37.6 5.1 %collective-permute-start = (bf16[3,512]{1,0:T(4,128)(2,1)S(1)}, bf16[3,512]{1,0:T(4,128)(2,1)S(1)}, u32[]{:S(2)}, u32[]{:S(2)}) collective-permute-start(bf16[3,512]{1,0:T(4,128)(2,1)S(1)} %slice.727), channel_id=1, source_target_pairs={{0,16},{16,32},{32,48},{48,64},{64,80},{80,96},{96,112},{112,128},... | collective-permute-start | bytes 9224 | tf_op jit(solution)/shard_map/ppermute | solution.py:27
  164.4 23.6 %copy-start.1 = (bf16[32,194,128]{2,1,0:T(8,128)(2,1)S(1)}, bf16[32,194,128]{2,1,0:T(8,128)(2,1)}, u32[]{:S(2)}) copy-start(bf16[32,194,128]{2,1,0:T(8,128)(2,1)} %all-gather.4.cloned.1.call-done) | copy-start | bytes 4767748
  184.4 2.9 copy-start.9
  184.4 4.0 %copy-start.7 = (f32[2,1,128,128]{3,2,1,0:T(8,128)S(1)}, f32[2,1,128,128]{3,2,1,0:T(8,128)}, u32[]{:S(2)}) copy-start(f32[2,1,128,128]{3,2,1,0:T(8,128)} %copy-done.6) | copy-start | bytes 393220
  184.4 4.4 %copy-start.8 = (bf16[256,128]{1,0:T(8,128)(2,1)S(1)}, bf16[256,128]{1,0:T(8,128)(2,1)}, u32[]{:S(2)}) copy-start(bf16[256,128]{1,0:T(8,128)(2,1)} %param.35) | copy-start | bytes 196612
  184.4 5.2 %copy-start.14 = (f32[128]{0:T(128)S(1)}, f32[128]{0:T(128)}, u32[]{:S(2)}) copy-start(f32[128]{0:T(128)} %param.45) | copy-start | bytes 1540
  188.4 1.7 copy-start.4
  188.4 1.7 copy-start.15
  212.6 7.4 %copy-start.12 = (f32[256,3]{0,1:T(4,128)S(1)}, f32[256,3]{0,1:T(4,128)}, u32[]{:S(2)}) copy-start(f32[256,3]{0,1:T(4,128)} %param.50) | copy-start | bytes 9220
  212.6 8.2 %copy-start.10 = (s32[256,3]{0,1:T(4,128)S(1)}, s32[256,3]{0,1:T(4,128)}, u32[]{:S(2)}) copy-start(s32[256,3]{0,1:T(4,128)} %param.49) | copy-start | bytes 9220
  212.6 21.3 %copy-start.2 = (bf16[256,2048]{1,0:T(8,128)(2,1)S(1)}, bf16[256,2048]{1,0:T(8,128)(2,1)}, u32[]{:S(2)}) copy-start(bf16[256,2048]{1,0:T(8,128)(2,1)} %param.29) | copy-start | bytes 3145732
  213.8 20.0 %all-to-all-start.1 = ((bf16[16,16,2048]{2,1,0:T(8,128)(2,1)}), bf16[16,16,2048]{2,1,0:T(8,128)(2,1)S(1)}, u32[]{:S(2)}, u32[]{:S(2)}) async-start(bf16[16,16,2048]{2,1,0:T(8,128)(2,1)} %broadcast_in_dim.38), calls=%async_computation.1 | async-start | bytes 2097152 | tf_op jit(solution)/shard_map/all_to_all | solution.py:102
Sparse Core Ops, SparseCore 0:
  37.7 75.3 all-gather.3

commit v2 on v1

--- a/solution.py
+++ b/solution.py
@@ -11,7 +11,7 @@
 NARROW_HEAD_DIM = 64
 WIDE_HEAD_DIM = 128
 GROUPS = 4
-BLOCK = 128
+CONV = 4
 SP = "sp"
 
 
@@ -21,199 +21,10 @@
 FULL_PRECISION = lax.Precision.HIGHEST
 
 
-def passed_along(block, axis, distance):
-    devices = range(lax.axis_size(axis))
-    route = [(i - distance, i) for i in devices if i - distance in devices]
-    return lax.ppermute(block, axis, route)
-
-
-def filled_with(x, identity):
-    return jax.tree.map(
-        lambda part, zero: jnp.zeros_like(part) + jnp.asarray(zero, part.dtype), x, identity
-    )
-
-
-def all_in_one(x, axis):
-    leaves = jax.tree.leaves(x)
-    turns = sorted(range(len(leaves)), key=lambda k: -leaves[k].size)
-    width = (1, *leaves[turns[0]].shape)[-1]
-    lines = [
-        jnp.pad(leaves[k].reshape(-1), (0, -leaves[k].size % width)).reshape(-1, width)
-        for k in turns
-    ]
-    both, at, found = (lax.all_gather(jnp.concatenate(lines), axis), 0, {})
-    for k, line in zip(turns, lines):
-        piece = both[:, at : at + len(line)].reshape(len(both), -1)
-        found[k] = piece[:, : leaves[k].size].reshape(-1, *leaves[k].shape)
-        at += len(line)
-    numbers = iter(range(len(leaves)))
-    return jax.tree.map(lambda _: found[next(numbers)], x)
-
-
-def entering_2(x, axes, combine, identity):
-    before = start = filled_with(x, identity)
-    running = x
-    for axis in (axes,):
-        length, mine = (lax.axis_size(axis), lax.axis_index(axis))
-        pieces = all_in_one(
-            jax.tree.map(
-                lambda part, kind: part.astype(kind),
-                running,
-                jax.tree.map(lambda a: jnp.bfloat16 if a.dtype == jnp.float32 else a.dtype, x),
-            ),
-            axis,
-        )
-        inside, running = (start, start)
-        for k in range(length):
-            passed = k < mine
-            running = combine(
-                running, jax.tree.map(lambda part, own: part[k].astype(own.dtype), pieces, x)
-            )
-            inside = jax.tree.map(lambda new, old: jnp.where(passed, new, old), running, inside)
-        before = combine(inside, before)
-    return before
-
-
-def split_up(x, dim, length):
-    lengths = x.shape
-    parts = x.reshape(*lengths[:dim], length, lengths[dim] // length, *lengths[dim + 1 :])
-    return jnp.moveaxis(parts, dim, 0)
-
-
-def sent_and_summed(x, axis, dim):
-    length = lax.axis_size(axis)
-    parts = lax.all_to_all(split_up(x, dim, length), axis, 0, 0, tiled=True)
-    return jnp.sum(parts.astype(jnp.float32), axis=0)
-
-
-def padded_to(lines, length):
-    spare = -len(lines) % length
-    return jnp.pad(lines, [(0, spare)] + [(0, 0)] * (lines.ndim - 1))
-
-
-def in_order(parts, dim):
-    parts = jnp.moveaxis(parts, 0, dim)
-    lengths = parts.shape
-    return parts.reshape(*lengths[:dim], lengths[dim] * lengths[dim + 1], *lengths[dim + 2 :])
-
-
-def from_everyone(x, axis):
-    copies = jnp.broadcast_to(x, (lax.axis_size(axis), *x.shape))
-    return lax.all_to_all(copies, axis, split_axis=0, concat_axis=0, tiled=True)
-
-
-def collect(x, axis, dim):
-    return in_order(from_everyone(x, axis), dim)
-
-
-def total_of(x, axes):
-    lines = x.reshape(-1, x.shape[-1])
-    own = sent_and_summed(padded_to(lines, lax.axis_size(axes)), axes, 0)
-    whole = collect(own.astype(jnp.bfloat16), axes, 0)
-    return whole[: len(lines)].reshape(x.shape).astype(jnp.float32)
-
-
-def conv_with_rim(values, rim_rows, weight):
-    length = values.shape[0]
-    padded = jnp.concatenate([rim_rows, values], axis=0).astype(jnp.float32)
-    accumulated = jnp.zeros((length, values.shape[1]), jnp.float32)
-    for tap_index in range(weight.shape[0]):
-        accumulated = accumulated + weight[tap_index] * padded[tap_index : tap_index + length]
-    return jax.nn.silu(accumulated)
-
-
-def pick_groups(channel_table, first_head, head_count):
-    length = channel_table.shape[0]
-    grouped = channel_table.reshape(length, GROUPS, -1)
-    owners = (first_head + jnp.arange(head_count, dtype=jnp.int32)) // (HEADS // GROUPS)
-    chooser = (owners[:, None] == jnp.arange(GROUPS, dtype=jnp.int32)[None, :]).astype(jnp.float32)
-    return jnp.einsum("sgn,hg->shn", grouped, chooser, precision=FULL_PRECISION)
-
-
-def local_head(values, step_logarithm, key_head_rows, query_head_rows, block_len):
-    block_count = values.shape[0] // block_len
-    values = values.reshape(block_count, block_len, -1)
-    step_logarithm = step_logarithm.reshape(block_count, block_len)
-    key_head_rows = key_head_rows.reshape(block_count, block_len, -1)
-    query_head_rows = query_head_rows.reshape(block_count, block_len, -1)
-    cum_decay = jnp.cumsum(step_logarithm, axis=1)
-    causal_mask = jnp.arange(block_len)[:, None] >= jnp.arange(block_len)[None, :]
-    decay_gaps = jnp.where(causal_mask[None], cum_decay[:, :, None] - cum_decay[:, None, :], -1e30)
-    scores = jnp.einsum(
-        "bln,bsn->bls", query_head_rows, key_head_rows, precision=FULL_PRECISION
-    ) * jnp.exp(decay_gaps)
-    inside = jnp.einsum("bls,bsp->blp", scores, values, precision=FULL_PRECISION)
-    tail_decay = jnp.exp(cum_decay[:, -1:] - cum_decay)
-    states = jnp.einsum(
-        "bln,blp->bnp", key_head_rows * tail_decay[..., None], values, precision=FULL_PRECISION
-    )
-    totals = cum_decay[:, -1]
-
-    def walk(running, member):
-        return (jnp.exp(member[1]) * running + member[0], running)
-
-    closing, entering = lax.scan(walk, jnp.zeros(states.shape[1:], jnp.float32), (states, totals))
-    before = jnp.cumsum(totals) - totals
-    return (inside, entering, closing, jnp.sum(totals), before, cum_decay, query_head_rows)
-
-
-def finish_head(inside, entering, before, cum_decay, query_blocks, carried):
-    starting = entering + jnp.exp(before)[:, None, None] * carried[None]
-    readout = jnp.einsum(
-        "bln,bnp->blp",
-        query_blocks * jnp.exp(cum_decay)[..., None],
-        starting,
-        precision=FULL_PRECISION,
-    )
-    return (inside + readout).reshape(-1, inside.shape[-1])
-
-
-def group_out(scanned, mixed_input_rows, direct_input_term, gate_input_rows, norm_gain_vector):
-    length, head_count, head_dimension = mixed_input_rows.shape
-    gated = jax.nn.silu(gate_input_rows.astype(jnp.float32)).reshape(
-        length, head_count, head_dimension
-    )
-    result = (scanned + direct_input_term[None, :, None] * mixed_input_rows) * gated
-    result = result * lax.rsqrt(jnp.mean(result * result, axis=-1, keepdims=True) + NORM_EPS)
-    return (result.reshape(length, head_count * head_dimension) * norm_gain_vector).astype(
-        jnp.bfloat16
-    )
-
-
-def head_pieces_list(
-    mixed_input_rows,
-    step_length_values,
-    decay_vector,
-    position_decay_rows,
-    key_head_rows,
-    query_head_rows,
-):
-    step_logarithm = -jnp.exp(decay_vector)[None, :] * step_length_values + position_decay_rows
-    values = mixed_input_rows * step_length_values[..., None]
-    walker = functools.partial(local_head, block_len=BLOCK)
-    return jax.vmap(walker, in_axes=(1, 1, 1, 1))(
-        values, step_logarithm, key_head_rows, query_head_rows
-    )
-
-
-def finish_group(parts, carried_states):
-    return jax.vmap(finish_head, in_axes=(0, 0, 0, 0, 0, 0), out_axes=1)(
-        parts[0], parts[1], parts[4], parts[5], parts[6], carried_states
-    )
-
-
-def chain_combine(earlier, later):
-    return (
-        earlier[0] + later[0],
-        earlier[1] + later[1],
-        jnp.exp(later[0])[:, None, None] * earlier[2] + later[2],
-        jnp.exp(later[1])[:, None, None] * earlier[3] + later[3],
-    )
-
-
 MESH = pl.DeviceIdType.MESH
 CORES = 2
 SIDE = 4
+LAG = 2
 
 
 def remote(src, dst, send_sem, recv_sem, device):
@@ -598,10 +409,9 @@
 
     plans = [steps(u) for u in range(units)]
     depth = len(plans[0][0])
-    for tick in range(units + depth - 1):
-        for u in range(units):
-            if 0 <= tick - u < depth:
-                plans[u][0][tick - u]()
+    turns = sorted((u + LAG * k, -k, u) for u in range(units) for k in range(depth))
+    for _, k, u in turns:
+        plans[u][0][-k]()
     for copy in returns.values():
         copy.wait_recv()
     combined = state[...] + dot(share[0], back[...]) + dot(share[1], back[...])
@@ -659,6 +469,386 @@
     )(normed, state, routes, routes.T, weights, gate, up, down)
 
 
+def fine_dot(a, b, dims=(((1,), (0,)), ((), ()))):
+    return lax.dot_general(
+        a, b, dims, precision=FULL_PRECISION, preferred_element_type=jnp.float32
+    )
+
+
+def in_three(x):
+    high, rest = x.astype(jnp.bfloat16), None
+    rest = x - high.astype(jnp.float32)
+    middle = rest.astype(jnp.bfloat16)
+    low = (rest - middle.astype(jnp.float32)).astype(jnp.bfloat16)
+    return high, middle, low
+
+
+def silu(x):
+    return x * jax.nn.sigmoid(x)
+
+
+RIM = 16
+STATE_ROWS = 8
+
+
+def mixer_kernel(
+    chips,
+    narrow_in,
+    wide_in,
+    narrow_gate,
+    wide_gate,
+    columns,
+    lines,
+    narrow_taps,
+    wide_taps,
+    key_taps,
+    query_taps,
+    narrow_gain,
+    wide_gain,
+    last_gain,
+    key_hbm,
+    query_hbm,
+    resid_hbm,
+    narrow_rows_hbm,
+    wide_rows_hbm,
+    normed_out,
+    state_out,
+    keys,
+    queries,
+    resid,
+    narrow_rows,
+    wide_rows,
+    narrow_rim,
+    wide_rim,
+    key_rim,
+    query_rim,
+    padded,
+    told,
+    heard,
+    answer,
+    carried,
+    partial,
+    relay,
+    sums,
+    half,
+    last,
+    squares_out,
+    squares,
+    load_sem,
+    rim_sent,
+    rim_got,
+    told_sent,
+    told_got,
+    answer_sent,
+    answer_got,
+    sum_sent,
+    sum_got,
+    square_sent,
+    square_got,
+):
+    place = Place(chips)
+    devices = chips * CORES
+    length = narrow_in.shape[0]
+    width = keys.shape[1]
+    plane = SIDE * SIDE
+    barrier = pltpu.get_barrier_semaphore()
+    count = 0
+    for step in range(1, plane):
+        pl.semaphore_signal(
+            barrier, inc=1, device_id=(place.sp, (place.tp + step) % plane), device_id_type=MESH
+        )
+        count += 1
+    for step in range(1, devices):
+        pl.semaphore_signal(
+            barrier, inc=1, device_id=((place.sp + step) % devices, place.tp), device_id_type=MESH
+        )
+        count += 1
+    group = pl.multiple_of((place.tp // (HEADS // GROUPS)) * width, width)
+    mine = pl.ds(pl.multiple_of(place.tp * width, width), width)
+    pairs = (
+        (key_hbm.at[:, pl.ds(group, width)], keys),
+        (query_hbm.at[:, pl.ds(group, width)], queries),
+        (resid_hbm.at[:, mine], resid),
+        (narrow_rows_hbm, narrow_rows),
+        (wide_rows_hbm, wide_rows),
+    )
+    loads = [pltpu.make_async_copy(src, dst, load_sem.at[k]) for k, (src, dst) in enumerate(pairs)]
+    for load in loads:
+        load.start()
+
+    upper = ones_where(iota((length, length), 0) <= iota((length, length), 1))
+    causal = iota((length, length), 0) >= iota((length, length), 1)
+    lower = ones_where(causal)
+    tall, flat = columns[...], lines[...]
+    tall_sum = sum(dot(lower, piece) for piece in in_three(tall))
+    flat_sum = sum(dot(piece, upper) for piece in in_three(flat))
+    decay, tails, totals, steps = [], [], [], []
+    for kind in (0, 1):
+        down_column = tall_sum[:, 2 + kind : 3 + kind]
+        across = flat_sum[2 + kind : 3 + kind, :]
+        decay.append(jnp.exp(jnp.where(causal, down_column - across, -1e30)))
+        total = down_column[length - 1 : length, :]
+        totals.append(total)
+        tails.append(jnp.exp(total - down_column))
+        steps.append(tall[:, kind : kind + 1])
+    fades = [jnp.exp(tall_sum[:, 2 + kind : 3 + kind]) for kind in (0, 1)]
+    rows = iota((width, devices * STATE_ROWS), 0)
+    spots = iota((width, devices * STATE_ROWS), 1)
+    per = STATE_ROWS // 2
+    owner_row = (spots >> 3) * per + (spots & (per - 1))
+    wide_spread = jnp.where((owner_row == rows) & ((spots & 7) < per), 1.0, 0.0)
+    narrow_spread = jnp.where((owner_row == rows) & ((spots & 7) >= per), 1.0, 0.0)
+
+    loads[0].wait()
+    loads[1].wait()
+    pl.semaphore_wait(barrier, count)
+    following = ((place.sp + 1) % devices, place.tp)
+    rims = []
+    tail = pl.ds(length - RIM, RIM)
+    for k, (src, dst) in enumerate(
+        ((narrow_in, narrow_rim), (wide_in, wide_rim), (keys, key_rim), (queries, query_rim))
+    ):
+        copy = remote(src.at[tail], dst, rim_sent.at[k], rim_got.at[k], following)
+        copy.start()
+        rims.append(copy)
+    for copy in rims:
+        copy.wait_recv()
+
+    inner = place.sp > 0
+
+    def mixed_rows(values, rim, taps):
+        size = values.shape[1]
+        before = jnp.where(inner, rim[...].astype(jnp.float32), 0.0)
+        padded[0:RIM, 0:size] = before
+        padded[RIM : RIM + length, 0:size] = values[...].astype(jnp.float32)
+        total = jnp.zeros((length, size), jnp.float32)
+        for k in range(CONV):
+            start = RIM - CONV + 1 + k
+            total = total + taps[k : k + 1, :] * padded[start : start + length, 0:size]
+        return silu(total)
+
+    key = mixed_rows(keys, key_rim, key_taps[:, pl.ds(group, width)])
+    query = mixed_rows(queries, query_rim, query_taps[:, pl.ds(group, width)])
+    narrow_mix = mixed_rows(narrow_in, narrow_rim, narrow_taps[...])
+    wide_mix = mixed_rows(wide_in, wide_rim, wide_taps[...])
+    narrow_size = narrow_mix.shape[1]
+    narrow_value, wide_value = narrow_mix * steps[0], wide_mix * steps[1]
+
+    turned = (((0,), (0,)), ((), ()))
+    wide_keys = fine_dot(key, wide_spread)
+    narrow_keys = fine_dot(key, narrow_spread)
+    wide_state = fine_dot(wide_keys, wide_value * tails[1], turned)
+    narrow_state = fine_dot(
+        narrow_keys,
+        jnp.concatenate(
+            [narrow_value * tails[0], jnp.zeros((length, width - narrow_size), jnp.float32)], axis=1
+        ),
+        turned,
+    )
+    tile = iota((devices * STATE_ROWS, width), 0) & 7
+    lane = iota((devices * STATE_ROWS, width), 1)
+    spare = jnp.where(lane < (narrow_size + width) // 2, totals[1], totals[0])
+    message = wide_state + narrow_state
+    message = jnp.where((tile >= per) & (lane >= narrow_size), spare, message)
+    told[...] = message.reshape(devices, STATE_ROWS, width).astype(jnp.bfloat16)
+
+    def exchange(src, dst, sent, got):
+        copies = []
+        dst[place.sp] = src[place.sp]
+        for step in range(1, devices):
+            other = (place.sp + step) % devices
+            copy = remote(
+                src.at[other], dst.at[place.sp], sent.at[step], got.at[step], (other, place.tp)
+            )
+            copy.start()
+            copies.append(copy)
+        return copies
+
+    tells = exchange(told, heard, told_sent, told_got)
+
+    scores = fine_dot(query, key, (((1,), (1,)), ((), ())))
+    narrow_inside = fine_dot(scores * decay[0], narrow_value)
+    wide_inside = fine_dot(scores * decay[1], wide_value)
+    wide_query = fine_dot(query * fades[1], wide_spread)
+    narrow_query = fine_dot(query * fades[0], narrow_spread)
+    narrow_open, wide_open = silu(narrow_gate[...].astype(jnp.float32)), silu(
+        wide_gate[...].astype(jnp.float32)
+    )
+
+    for copy in tells:
+        copy.wait_recv()
+    running = jnp.zeros((STATE_ROWS, width), jnp.float32)
+    upper_rows = iota((STATE_ROWS, width), 0) < per
+    for source in range(devices):
+        answer[source] = running.astype(jnp.bfloat16)
+        piece = heard[source].astype(jnp.float32)
+        wide_total = piece[per : per + 1, narrow_size : narrow_size + 1]
+        middle = (narrow_size + width) // 2
+        narrow_total = piece[per : per + 1, middle : middle + 1]
+        factor = jnp.exp(jnp.where(upper_rows, wide_total, narrow_total))
+        running = factor * running + piece
+    answers = exchange(answer, carried, answer_sent, answer_got)
+
+    for load in loads[2:]:
+        load.wait()
+    for copy in answers:
+        copy.wait_recv()
+    entering = carried[...].astype(jnp.float32).reshape(devices * STATE_ROWS, width)
+
+    def head(inside, asked, size, kind, mix, opened, gain):
+        result = inside + fine_dot(asked, entering)[:, :size]
+        result = (result + tall[:, 4 + kind : 5 + kind] * mix) * opened
+        mean = jnp.sum(result * result, axis=-1, keepdims=True) * (1.0 / size)
+        return (result * lax.rsqrt(mean + NORM_EPS) * gain[...]).astype(jnp.bfloat16)
+
+    narrow = head(narrow_inside, narrow_query, narrow_size, 0, narrow_mix, narrow_open, narrow_gain)
+    wide = head(wide_inside, wide_query, width, 1, wide_mix, wide_open, wide_gain)
+
+    totals_of = [
+        Summer(
+            place, first, partial.at[u], relay.at[u], sums.at[u], half.at[u], last.at[u],
+            sum_sent.at[u], sum_got.at[u],
+        )
+        for u, first in ((0, "x"), (1, "y"))
+    ]
+    unit = length // 2
+    for i in range(SIDE):
+        part = pl.ds(i * SIDE * width, SIDE * width)
+        product = dot(narrow, narrow_rows[:, part]) + dot(wide, wide_rows[:, part])
+        product = product.astype(jnp.bfloat16)
+        for j in range(SIDE):
+            for u in (0, 1):
+                partial[u, i, j] = product[u * unit : (u + 1) * unit, j * width : (j + 1) * width]
+    for move in ("open", "pass_on", "turn", "pass_again"):
+        for total in totals_of:
+            getattr(total, move)()
+    mixed = jnp.concatenate([total.close() for total in totals_of], axis=0)
+    hidden = resid[...].astype(jnp.float32) + mixed
+    state_out[...] = hidden
+    ones = jnp.ones((8, width), jnp.float32)
+    own = fine_dot(ones, hidden * hidden, (((1,), (1,)), ((), ())))[0:1, :]
+    squares_out[...] = own
+    squares[place.tp] = own
+    shares = []
+    for step in range(1, plane):
+        other = (place.tp + step) % plane
+        copy = remote(
+            squares_out, squares.at[place.tp], square_sent.at[step], square_got.at[step],
+            (place.sp, other),
+        )
+        copy.start()
+        shares.append(copy)
+    for copy in shares:
+        copy.wait_recv()
+    whole = squares[0]
+    for k in range(1, plane):
+        whole = whole + squares[k]
+    diagonal = iota((length, length), 0) == iota((length, length), 1)
+    mean = jnp.sum(jnp.where(diagonal, whole, 0.0), axis=1, keepdims=True) * (1.0 / (plane * width))
+    normed_out[...] = (
+        hidden * lax.rsqrt(mean + NORM_EPS) * last_gain[:, mine]
+    ).astype(jnp.bfloat16)
+    for copy in rims + tells + answers + shares:
+        copy.wait_send()
+    for total in totals_of:
+        for copy in total.started:
+            copy.wait_send()
+
+
+def mixer_layer(
+    narrow_in,
+    wide_in,
+    narrow_gate,
+    wide_gate,
+    columns,
+    narrow_taps,
+    wide_taps,
+    key_taps,
+    query_taps,
+    narrow_gain,
+    wide_gain,
+    last_gain,
+    key_in,
+    query_in,
+    resid,
+    narrow_rows,
+    wide_rows,
+    chips,
+):
+    length, width = wide_in.shape
+    devices = chips * CORES
+    plane = SIDE * SIDE
+    unit = length // 2
+    bf16, f32 = jnp.bfloat16, jnp.float32
+    vmem, any_ = pl.BlockSpec(memory_space=pltpu.VMEM), pl.BlockSpec(memory_space=pl.ANY)
+    dma = pltpu.SemaphoreType.DMA
+    return pl.pallas_call(
+        functools.partial(mixer_kernel, chips),
+        out_shape=(
+            jax.ShapeDtypeStruct((length, width), bf16),
+            jax.ShapeDtypeStruct((length, width), f32),
+        ),
+        in_specs=[vmem] * 13 + [any_] * 5,
+        out_specs=(vmem, vmem),
+        scratch_shapes=[
+            pltpu.VMEM((length, width), bf16),
+            pltpu.VMEM((length, width), bf16),
+            pltpu.VMEM((length, width), bf16),
+            pltpu.VMEM(narrow_rows.shape, bf16),
+            pltpu.VMEM(wide_rows.shape, bf16),
+            pltpu.VMEM((RIM, narrow_in.shape[1]), bf16),
+            pltpu.VMEM((RIM, width), bf16),
+            pltpu.VMEM((RIM, width), bf16),
+            pltpu.VMEM((RIM, width), bf16),
+            pltpu.VMEM((RIM + length, width), f32),
+            pltpu.VMEM((devices, STATE_ROWS, width), bf16),
+            pltpu.VMEM((devices, STATE_ROWS, width), bf16),
+            pltpu.VMEM((devices, STATE_ROWS, width), bf16),
+            pltpu.VMEM((devices, STATE_ROWS, width), bf16),
+            pltpu.VMEM((2, SIDE, SIDE, unit, width), bf16),
+            pltpu.VMEM((2, 2, SIDE, unit // 2, width), bf16),
+            pltpu.VMEM((2, 2, SIDE, unit, width), bf16),
+            pltpu.VMEM((2, 2, unit // 2, width), bf16),
+            pltpu.VMEM((2, 2, unit, width), bf16),
+            pltpu.VMEM((1, length), f32),
+            pltpu.VMEM((plane, 1, length), f32),
+            dma((5,)),
+            dma((4,)),
+            dma((4,)),
+            dma((devices,)),
+            dma((devices,)),
+            dma((devices,)),
+            dma((devices,)),
+            dma((2, 8)),
+            dma((2, 8)),
+            dma((plane,)),
+            dma((plane,)),
+        ],
+        compiler_params=pltpu.CompilerParams(
+            collective_id=0, has_side_effects=True, vmem_limit_bytes=56 * 1024 * 1024
+        ),
+    )(
+        narrow_in,
+        wide_in,
+        narrow_gate,
+        wide_gate,
+        columns,
+        columns.T,
+        narrow_taps,
+        wide_taps,
+        key_taps,
+        query_taps,
+        narrow_gain.reshape(1, -1),
+        wide_gain.reshape(1, -1),
+        last_gain.reshape(1, -1),
+        key_in,
+        query_in,
+        resid,
+        narrow_rows,
+        wide_rows,
+    )
+
+
 def local(
     resid,
     narrow_head_input,
@@ -686,93 +876,31 @@
     expert_up_matrix,
     expert_down_matrix,
 ):
-    length = resid.shape[0]
-    head_count = narrow_head_input.shape[1] // NARROW_HEAD_DIM
-    rim_len = narrow_conv_taps.shape[0] - 1
-    rim_rows = passed_along(
-        (
-            narrow_head_input[length - rim_len :],
-            wide_head_input[length - rim_len :],
-            key_group_input[length - rim_len :],
-            query_group_input[length - rim_len :],
-        ),
-        SP,
-        1,
+    chips = lax.axis_size(SP) // CORES
+    steps = jax.nn.softplus(step_input_rows[:, :, 0].astype(jnp.float32))
+    decays = -jnp.exp(head_decay_logarithm[:, 0])[None, :] * steps + position_log_decay[:, :, 0]
+    direct = jnp.broadcast_to(direct_input_weight[:, 0][None, :], steps.shape)
+    columns = jnp.concatenate([steps, decays, direct, jnp.zeros_like(direct)], axis=1)
+    own_columns, own_state = mixer_layer(
+        narrow_head_input,
+        wide_head_input,
+        narrow_output_gate,
+        wide_output_gate,
+        columns,
+        narrow_conv_taps,
+        wide_conv_taps,
+        key_conv_taps,
+        query_conv_taps,
+        narrow_norm_gain,
+        wide_norm_gain,
+        feedforward_norm_gain,
+        key_group_input,
+        query_group_input,
+        resid,
+        narrow_output_rows,
+        wide_output_rows,
+        chips,
     )
-    narrow_head_mix = conv_with_rim(narrow_head_input, rim_rows[0], narrow_conv_taps).reshape(
-        length, head_count, NARROW_HEAD_DIM
-    )
-    wide_head_mix = conv_with_rim(wide_head_input, rim_rows[1], wide_conv_taps).reshape(
-        length, head_count, WIDE_HEAD_DIM
-    )
-    first_head = lax.axis_index("tp") * head_count
-    key_head_rows = pick_groups(
-        conv_with_rim(key_group_input, rim_rows[2], key_conv_taps), first_head, head_count
-    )
-    query_head_rows = pick_groups(
-        conv_with_rim(query_group_input, rim_rows[3], query_conv_taps), first_head, head_count
-    )
-    step_length_values = jax.nn.softplus(step_input_rows.astype(jnp.float32))
-    narrow_parts = head_pieces_list(
-        narrow_head_mix,
-        step_length_values[:, 0],
-        head_decay_logarithm[0],
-        position_log_decay[:, 0],
-        key_head_rows,
-        query_head_rows,
-    )
-    wide_parts = head_pieces_list(
-        wide_head_mix,
-        step_length_values[:, 1],
-        head_decay_logarithm[1],
-        position_log_decay[:, 1],
-        key_head_rows,
-        query_head_rows,
-    )
-    summary = (narrow_parts[3], wide_parts[3], narrow_parts[2], wide_parts[2])
-    carried = entering_2(
-        summary,
-        SP,
-        chain_combine,
-        (
-            jnp.zeros_like(summary[0]),
-            jnp.zeros_like(summary[1]),
-            jnp.zeros_like(summary[2]),
-            jnp.zeros_like(summary[3]),
-        ),
-    )
-    narrow_carry, wide_carry = (carried[2], carried[3])
-    narrow_head_output = group_out(
-        finish_group(narrow_parts, narrow_carry),
-        narrow_head_mix,
-        direct_input_weight[0],
-        narrow_output_gate,
-        narrow_norm_gain,
-    )
-    wide_head_output = group_out(
-        finish_group(wide_parts, wide_carry),
-        wide_head_mix,
-        direct_input_weight[1],
-        wide_output_gate,
-        wide_norm_gain,
-    )
-    partial_mix = jnp.dot(
-        narrow_head_output, narrow_output_rows, preferred_element_type=jnp.float32
-    )
-    partial_mix = partial_mix + jnp.dot(
-        wide_head_output, wide_output_rows, preferred_element_type=jnp.float32
-    )
-    mixed = total_of(partial_mix.astype(jnp.bfloat16), "tp")
-    hidden_state = resid.astype(jnp.float32) + mixed
-    normed = (
-        hidden_state
-        * lax.rsqrt(jnp.mean(hidden_state * hidden_state, axis=-1, keepdims=True) + NORM_EPS)
-        * feedforward_norm_gain
-    ).astype(jnp.bfloat16)
-    column_width = normed.shape[1] // lax.axis_size("tp")
-    tp_index = lax.axis_index("tp")
-    own_columns = lax.dynamic_slice_in_dim(normed, tp_index * column_width, column_width, 1)
-    own_state = lax.dynamic_slice_in_dim(hidden_state, tp_index * column_width, column_width, 1)
     return expert_layer(
         own_columns,
         own_state,
@@ -781,7 +909,7 @@
         expert_gate_matrix[0],
         expert_up_matrix[0],
         expert_down_matrix[0],
-        lax.axis_size(SP) // CORES,
+        chips,
         2,
     )
 

time: 340 us -> 156 us (0.46)
  waiting for transfers between devices: 79.6 us -> 0 us
  between operations: 58 us -> 0.04 us
  Pallas kernels: 93.1 us -> 146 us
  local copies, waits for them, and re-layouts: 40.4 us -> 6.08 us
  blocking collectives: 22 us -> 0 us
  starting transfers between devices: 17.8 us -> 0 us
  other arithmetic: 19.8 us -> 2.1 us
  matrix products: 5.68 us -> 0 us
    all_gather x1 -> x0, waiting for transfers between devices: 68.1 us -> none  [all_in_one(): both, at, found = (lax.all_gather(jnp.concatenate(lines), axis), 0, {})]
    pallas_call x0 -> x1, Pallas kernels: none -> 63.7 us  [mixer_layer(): pl.pallas_call(functools.partial(mixer_kernel, chips), out_shape=(jax.Sha...]
    all_to_all x1 -> x0, blocking collectives: 22 us -> none  [sent_and_summed(): parts = lax.all_to_all(split_up(x, dim, length), axis, 0, 0, tiled=True)]
    convert_element_type x24 -> x0, local copies, waits for them, and re-layouts: 20.6 us -> none  [entering_2(): part[k].astype(own.dtype)]
    ppermute x4 -> x0, starting transfers between devices: 11.7 us -> none  [passed_along(): return lax.ppermute(block, axis, route)]
    all_to_all x1 -> x0, waiting for transfers between devices: 11.5 us -> none  [from_everyone(): return lax.all_to_all(copies, axis, split_axis=0, concat_axis=0, tiled=True)]
    pallas_call x1, Pallas kernels: 93.1 us -> 81.8 us  [expert_layer(): pl.pallas_call(functools.partial(expert_kernel, chips, cap, unit_chips),...]
    slice x13 -> x0, local copies, waits for them, and re-layouts: 8.64 us -> none  [the longest x4 2.62 us: entering_2(): part[k].astype(own.dtype)]
  transfers between devices with their start and end apart: 6 -> 0, of which waited for: 2 -> 0; matrix products, arithmetic and copies ran while one was open for 5% -> 0% of each run, Pallas kernels for 0% -> 0%
where the time goes in v2:
time: 156 us; the launch traced here: 154 us
  Pallas kernels  146 us (94%)
  local copies, waits for them, and re-layouts  6.08 us (4%)
  other arithmetic  2.1 us (1%)
    pallas_call x1, Pallas kernels, expert_layer(): pl.pallas_call(functools.partial(expert_kernel, chips, cap, unit_chips),...  81.8 us
    pallas_call x1, Pallas kernels, mixer_layer(): pl.pallas_call(functools.partial(mixer_kernel, chips), out_shape=(jax.Sha...  63.7 us
    unnamed x13, local copies, waits for them, and re-layouts  4.56 us

profile of v2, /device:TPU:6, one launch (start us, length us, event | category | flops | bytes accessed | tf_op | source)
XLA Modules:
  0.0 153.7 jit_solution(3360323925510097315)
XLA Ops:
  0.0 0.0 copy-start
  0.0 0.7 negate_bitcast_fusion
  0.7 0.7 pad.2.clone
  1.4 0.8 compare_select_fusion
  2.2 0.7 fusion.4
  2.8 0.0 copy-done
  2.8 0.0 copy-start.1
  2.8 0.7 copy.26.narrow_in
  3.6 0.0 copy-done.1
  3.6 0.7 copy.27.narrow_gate
  4.3 0.8 copy.28.columns
  5.1 0.0 copy-start.3
  5.1 63.7 %shard_map.235 = (bf16[256,128]{1,0:T(8,128)(2,1)}, f32[256,128]{1,0:T(8,128)}) custom-call(bf16[256,64]{1,0:T(8,128)(2,1)} %copy.26.narrow_in, bf16[256,128]{1,0:T(8,128)(2,1)} %wide_in.1, bf16[256,64]{1,0:T(8,128)(2,1)} %copy.27.narrow_gate, bf16[256,128]{1,0:T(8,128)(2,1)} %wide_gate.1, f32[256,8]{1,0:T(8,128)} %copy.28.columns, ...), custom_call_target="tpu_custom_call" | custom-call | tf_op jit(solution)/shard_map/pallas_call | solution.py:785
  68.8 0.0 copy-done.3
  68.8 0.0 copy-start.2
  68.8 0.8 copy.30.weights
  69.6 0.0 copy-done.2
  69.6 0.8 copy.29.routes
  70.4 81.8 %shard_map.236 = bf16[256,128]{1,0:T(8,128)(2,1)} custom-call(bf16[256,128]{1,0:T(8,128)(2,1)} %get-tuple-element.7.normed, f32[256,128]{1,0:T(8,128)} %get-tuple-element.8.state, s32[256,3]{1,0:T(8,128)} %copy.29.routes, s32[3,256]{1,0:T(4,128)} %bitcast.22, f32[256,3]{1,0:T(8,128)} %copy.30.weights, bf16[2048,128]{1,0:T(8,128)(2,1)} %bitcast.19, ...), custom_call_target="tpu_custom_call" | custom-call | tf_op jit(solution)/shard_map/pallas_call | solution.py:437
  152.3 1.5 copy.34
  (1 shorter events, 0.0 us)
Async XLA Ops:
  0.0 2.8 %copy-start = (bf16[256,64]{0,1:T(8,128)(2,1)S(1)}, bf16[256,64]{0,1:T(8,128)(2,1)}, u32[]{:S(2)}) copy-start(bf16[256,64]{0,1:T(8,128)(2,1)} %param.26) | copy-start | bytes 98308
  2.8 0.8 copy-start.1
  5.1 63.7 %copy-start.3 = (f32[256,3]{0,1:T(4,128)S(1)}, f32[256,3]{0,1:T(4,128)}, u32[]{:S(2)}) copy-start(f32[256,3]{0,1:T(4,128)} %param.46) | copy-start | bytes 9220
  68.8 0.8 copy-start.2

commit v3 on v2

--- a/solution.py
+++ b/solution.py
@@ -25,6 +25,7 @@
 CORES = 2
 SIDE = 4
 LAG = 2
+CHUNKS = 4
 
 
 def remote(src, dst, send_sem, recv_sem, device):
@@ -68,21 +69,130 @@
 def greet(place):
     barrier = pltpu.get_barrier_semaphore()
     count = 0
-    for axis in ("x", "y"):
-        for step in (1, SIDE - 1):
-            pl.semaphore_signal(barrier, inc=1, device_id=place.plane(axis, step), device_id_type=MESH)
+    devices = place.chips * CORES
+    for step in range(devices):
+        for side in range(SIDE):
+            if step or side:
+                device = (
+                    (place.sp + step) % devices,
+                    place.at["y"] * SIDE + (place.at["x"] + side) % SIDE,
+                )
+                pl.semaphore_signal(barrier, inc=1, device_id=device, device_id_type=MESH)
+                count += 1
+    for step in range(1, SIDE):
+        for side in range(SIDE):
+            device = (place.sp, ((place.at["y"] + step) % SIDE) * SIDE + (place.at["x"] + side) % SIDE)
+            pl.semaphore_signal(barrier, inc=1, device_id=device, device_id_type=MESH)
             count += 1
-    for step in range(place.chips):
-        if step:
-            pl.semaphore_signal(
-                barrier, inc=1, device_id=place.along(step, place.core), device_id_type=MESH
-            )
-            count += 1
-        pl.semaphore_signal(
-            barrier, inc=1, device_id=place.along(step, 1 - place.core), device_id_type=MESH
+    return barrier, count
+
+
+class Gather:
+    def __init__(self, place, gate_up, down, sent, got):
+        self.place, self.gate_up, self.down = place, gate_up, down
+        self.sent, self.got, self.started, self.loads = sent, got, {}, []
+        self.width = down.shape[0] // SIDE
+
+    def piece(self, kind, step, part=None):
+        index = self.place.index("x", step)
+        if kind == 2:
+            ref = self.down.at[pl.ds(pl.multiple_of(index * self.width, self.width), self.width)]
+        else:
+            start = pl.multiple_of(index * self.width + kind * SIDE * self.width, self.width)
+            ref = self.gate_up.at[:, pl.ds(start, self.width)]
+        if part is None:
+            return ref
+        size = ref.shape[0] // 2
+        return ref.at[pl.ds(part * size, size)]
+
+    def load(self, gate_hbm, up_hbm, down_hbm, sem):
+        for kind, src in enumerate((gate_hbm, up_hbm, down_hbm)):
+            copy = pltpu.make_async_copy(src, self.piece(kind, 0), sem.at[kind])
+            copy.start()
+            self.loads.append(copy)
+
+    def send(self, ref, kind, number, step):
+        copy = remote(
+            ref, ref, self.sent.at[kind, number], self.got.at[kind, number],
+            self.place.plane("x", step),
         )
-        count += 1
-    return barrier, count
+        copy.start()
+        self.started[(kind, number)] = copy
+
+    def open(self):
+        for kind in range(3):
+            self.loads[kind].wait()
+            self.send(self.piece(kind, 0), kind, 0, 1)
+            self.send(self.piece(kind, 0), kind, 1, SIDE - 1)
+
+    def pass_on(self, kind):
+        self.started[(kind, 0)].wait_recv()
+        self.send(self.piece(kind, SIDE - 1, 0), kind, 2, 1)
+        self.started[(kind, 1)].wait_recv()
+        self.send(self.piece(kind, 1, 1), kind, 3, SIDE - 1)
+
+    def close(self):
+        for kind in range(3):
+            self.started[(kind, 2)].wait_recv()
+            self.started[(kind, 3)].wait_recv()
+
+
+class Line:
+    def __init__(self, place, tokens, blocks, relay, sums, sent, got):
+        self.place, self.tokens, self.blocks = place, tokens, blocks
+        self.relay, self.sums, self.sent, self.got = relay, sums, sent, got
+        self.started = []
+        rows = tokens.shape[2]
+        self.low, self.high = pl.ds(0, rows // 2), pl.ds(rows // 2, rows // 2)
+
+    def send(self, src, dst, step):
+        number = len(self.started)
+        copy = remote(
+            src, dst, self.sent.at[number], self.got.at[number], self.place.plane("y", step)
+        )
+        copy.start()
+        self.started.append(copy)
+
+    def open(self):
+        own = self.tokens.at[self.place.at["y"]]
+        self.send(own, own, 1)
+        self.send(own, own, SIDE - 1)
+
+    def pass_on(self):
+        for side, step in ((0, SIDE - 1), (1, 1)):
+            self.started[side].wait_recv()
+            part = self.low if side == 0 else self.high
+            ref = self.tokens.at[self.place.index("y", step)].at[:, part]
+            self.send(ref, ref, SIDE - step)
+
+    def arrived(self):
+        self.started[2].wait_recv()
+        self.started[3].wait_recv()
+
+    def give(self):
+        far = self.blocks.at[self.place.index("y", 2)]
+        self.send(far.at[:, self.low], self.relay.at[0], 1)
+        self.send(far.at[:, self.high], self.relay.at[1], SIDE - 1)
+
+    def add(self):
+        for side, step in ((0, 1), (1, SIDE - 1)):
+            part = self.low if side == 0 else self.high
+            self.started[4 + side].wait_recv()
+            near = self.blocks.at[self.place.index("y", step)]
+            piece = near.at[:, part]
+            piece[...] = (
+                piece[...].astype(jnp.float32) + self.relay[side].astype(jnp.float32)
+            ).astype(jnp.bfloat16)
+            self.send(near, self.sums.at[side], step)
+
+    def total(self):
+        self.started[6].wait_recv()
+        self.started[7].wait_recv()
+        return (
+            self.blocks[self.place.at["y"]].astype(jnp.float32)
+            + self.sums[0].astype(jnp.float32)
+            + self.sums[1].astype(jnp.float32)
+        )
 
 
 def chunk_of(ref, axis, index):
@@ -156,55 +266,6 @@
             + self.last[0].astype(jnp.float32)
             + self.last[1].astype(jnp.float32)
         )
-
-
-class Spreader:
-    def __init__(self, place, first, blocks, sent, got):
-        self.place, self.first, self.second = place, first, "y" if first == "x" else "x"
-        self.blocks, self.sent, self.got = blocks, sent, got
-        self.started = []
-        rows = blocks.shape[2]
-        self.low, self.high = pl.ds(0, rows // 2), pl.ds(rows // 2, rows // 2)
-
-    def send(self, ref, axis, step, number):
-        copy = remote(
-            ref, ref, self.sent.at[number], self.got.at[number], self.place.plane(axis, step)
-        )
-        copy.start()
-        self.started.append(copy)
-
-    def block(self, step):
-        line = chunk_of(self.blocks, self.second, self.place.at[self.second])
-        return line.at[self.place.index(self.first, step)]
-
-    def line(self, step):
-        return chunk_of(self.blocks, self.second, self.place.index(self.second, step))
-
-    def open(self):
-        self.send(self.block(0), self.first, 1, 0)
-        self.send(self.block(0), self.first, SIDE - 1, 1)
-
-    def pass_on(self):
-        self.started[0].wait_recv()
-        self.send(self.block(SIDE - 1).at[self.low], self.first, 1, 2)
-        self.started[1].wait_recv()
-        self.send(self.block(1).at[self.high], self.first, SIDE - 1, 3)
-
-    def turn(self):
-        self.started[2].wait_recv()
-        self.started[3].wait_recv()
-        self.send(self.line(0), self.second, 1, 4)
-        self.send(self.line(0), self.second, SIDE - 1, 5)
-
-    def pass_again(self):
-        self.started[4].wait_recv()
-        self.send(self.line(SIDE - 1).at[:, self.low], self.second, 1, 6)
-        self.started[5].wait_recv()
-        self.send(self.line(1).at[:, self.high], self.second, SIDE - 1, 7)
-
-    def close(self):
-        self.started[6].wait_recv()
-        self.started[7].wait_recv()
 
 
 def iota(shape, dim):
@@ -259,216 +320,6 @@
         share[part] = jnp.where(mine, dot(piece, spread), 0.0).astype(jnp.bfloat16)
 
 
-def expert_kernel(
-    chips,
-    cap,
-    unit_chips,
-    normed,
-    state,
-    routes,
-    routes_turned,
-    weights,
-    gate_hbm,
-    up_hbm,
-    down_hbm,
-    out,
-    choice,
-    share,
-    outgoing,
-    tokens,
-    gate_up,
-    down,
-    partial,
-    relay,
-    sums,
-    half,
-    last,
-    result,
-    back,
-    load_sem,
-    out_sent,
-    out_got,
-    spread_sent,
-    spread_got,
-    sum_sent,
-    sum_got,
-    back_sent,
-    back_got,
-):
-    place = Place(chips)
-    experts = chips * CORES
-    barrier, count = greet(place)
-    loads = [
-        pltpu.make_async_copy(gate_hbm, gate_up.at[:, pl.ds(0, gate_hbm.shape[1])], load_sem.at[0]),
-        pltpu.make_async_copy(
-            up_hbm, gate_up.at[:, pl.ds(gate_hbm.shape[1], gate_hbm.shape[1])], load_sem.at[1]
-        ),
-        pltpu.make_async_copy(down_hbm, down, load_sem.at[2]),
-    ]
-    for load in loads:
-        load.start()
-    routing_tables(experts, cap, routes, routes_turned, weights, choice, share)
-    outgoing[...] = dot(choice[...], normed[...]).astype(jnp.bfloat16)
-    pl.semaphore_wait(barrier, count)
-
-    order = chip_order(chips)
-    spot = {d: k for k, d in enumerate(order)}
-    y, x = place.at["y"], place.at["x"]
-
-    def slot_rows(number):
-        return pl.ds(pl.multiple_of(number * cap, cap), cap)
-
-    dispatch = {}
-    for d in order:
-        for other in (0, 1):
-            core = place.core if other == 0 else 1 - place.core
-            device = place.along((chips - d) % chips, core)
-            rows = slot_rows(device[0])
-            to = slot_rows(spot[d] * CORES + place.core)
-            if d == 0 and other == 0:
-                tokens[y, x, to, :] = outgoing[rows, :]
-                continue
-            number = spot[d] * CORES + other
-            copy = remote(
-                outgoing.at[rows],
-                tokens.at[y, x, to],
-                out_sent.at[number],
-                out_got.at[number],
-                device,
-            )
-            copy.start()
-            dispatch[(d, other)] = copy
-
-    unit = unit_chips * CORES * cap
-    units = chips // unit_chips
-    width = gate_hbm.shape[1]
-    returns = {}
-
-    def steps(u):
-        first = "x" if u % 2 == 0 else "y"
-        rows = pl.ds(u * unit, unit)
-        spread = Spreader(
-            place, first, tokens.at[:, :, rows], spread_sent.at[u], spread_got.at[u]
-        )
-        total = Summer(
-            place, first, partial.at[u], relay.at[u], sums.at[u], half.at[u], last.at[u],
-            sum_sent.at[u], sum_got.at[u],
-        )
-
-        def arrive():
-            for d in order[u * unit_chips : (u + 1) * unit_chips]:
-                for other in (0, 1):
-                    if (d, other) in dispatch:
-                        dispatch[(d, other)].wait_recv()
-            spread.open()
-
-        def compute():
-            spread.close()
-            if u == 0:
-                for load in loads:
-                    load.wait()
-            lines = jnp.concatenate(
-                [tokens[i, j, rows, :] for i in range(SIDE) for j in range(SIDE)], axis=1
-            )
-            both = dot(lines, gate_up[...])
-            gate = jnp.minimum(both[:, :width], CLAMP_LIMIT)
-            up = jnp.clip(both[:, width:], -CLAMP_LIMIT, CLAMP_LIMIT)
-            act = ((up + 1.0) * gate * jax.nn.sigmoid(SIGMOID_SCALE * gate)).astype(jnp.bfloat16)
-            for i in range(SIDE):
-                wide = dot(act, down[:, i * SIDE * width : (i + 1) * SIDE * width])
-                for j in range(SIDE):
-                    partial[u, i, j] = wide[:, j * width : (j + 1) * width].astype(jnp.bfloat16)
-            total.open()
-
-        def close():
-            result[u] = total.close().astype(jnp.bfloat16)
-            for k, d in enumerate(order[u * unit_chips : (u + 1) * unit_chips]):
-                for other in (0, 1):
-                    core = place.core if other == 0 else 1 - place.core
-                    piece = slot_rows(k * CORES + core)
-                    to = slot_rows(place.sp)
-                    if d == 0 and other == 0:
-                        back[to, :] = result[u, piece, :]
-                        continue
-                    number = spot[d] * CORES + other
-                    copy = remote(
-                        result.at[u, piece],
-                        back.at[to],
-                        back_sent.at[number],
-                        back_got.at[number],
-                        place.along(d, core),
-                    )
-                    copy.start()
-                    returns[(d, other)] = copy
-
-        plan = [
-            arrive, spread.pass_on, spread.turn, spread.pass_again, compute,
-            total.pass_on, total.turn, total.pass_again, close,
-        ]
-        return plan, spread, total
-
-    plans = [steps(u) for u in range(units)]
-    depth = len(plans[0][0])
-    turns = sorted((u + LAG * k, -k, u) for u in range(units) for k in range(depth))
-    for _, k, u in turns:
-        plans[u][0][-k]()
-    for copy in returns.values():
-        copy.wait_recv()
-    combined = state[...] + dot(share[0], back[...]) + dot(share[1], back[...])
-    out[...] = combined.astype(jnp.bfloat16)
-    for copy in list(dispatch.values()) + list(returns.values()):
-        copy.wait_send()
-    for _, spread, total in plans:
-        for copy in spread.started + total.started:
-            copy.wait_send()
-
-
-def expert_layer(normed, state, routes, weights, gate, up, down, chips, unit_chips):
-    length, width = normed.shape
-    experts = chips * CORES
-    picks = routes.shape[1]
-    cap = 4 * length * picks // (3 * experts)
-    features = gate.shape[0]
-    unit = unit_chips * CORES * cap
-    units = chips // unit_chips
-    slots = experts * cap
-    vmem, any_ = pl.BlockSpec(memory_space=pltpu.VMEM), pl.BlockSpec(memory_space=pl.ANY)
-    bf16 = jnp.bfloat16
-    return pl.pallas_call(
-        functools.partial(expert_kernel, chips, cap, unit_chips),
-        out_shape=jax.ShapeDtypeStruct((length, width), bf16),
-        in_specs=[vmem] * 5 + [any_] * 3,
-        out_specs=vmem,
-        scratch_shapes=[
-            pltpu.VMEM((slots, length), bf16),
-            pltpu.VMEM((2, length, slots), bf16),
-            pltpu.VMEM((slots, width), bf16),
-            pltpu.VMEM((SIDE, SIDE, slots, width), bf16),
-            pltpu.VMEM((features, 2 * gate.shape[1]), bf16),
-            pltpu.VMEM(down.shape, bf16),
-            pltpu.VMEM((units, SIDE, SIDE, unit, width), bf16),
-            pltpu.VMEM((units, 2, SIDE, unit // 2, width), bf16),
-            pltpu.VMEM((units, 2, SIDE, unit, width), bf16),
-            pltpu.VMEM((units, 2, unit // 2, width), bf16),
-            pltpu.VMEM((units, 2, unit, width), bf16),
-            pltpu.VMEM((units, unit, width), bf16),
-            pltpu.VMEM((slots, width), bf16),
-            pltpu.SemaphoreType.DMA((3,)),
-            pltpu.SemaphoreType.DMA((experts,)),
-            pltpu.SemaphoreType.DMA((experts,)),
-            pltpu.SemaphoreType.DMA((units, 8)),
-            pltpu.SemaphoreType.DMA((units, 8)),
-            pltpu.SemaphoreType.DMA((units, 8)),
-            pltpu.SemaphoreType.DMA((units, 8)),
-            pltpu.SemaphoreType.DMA((experts,)),
-            pltpu.SemaphoreType.DMA((experts,)),
-        ],
-        compiler_params=pltpu.CompilerParams(
-            collective_id=1, has_side_effects=True, vmem_limit_bytes=56 * 1024 * 1024
-        ),
-    )(normed, state, routes, routes.T, weights, gate, up, down)
-
-
 def fine_dot(a, b, dims=(((1,), (0,)), ((), ()))):
     return lax.dot_general(
         a, b, dims, precision=FULL_PRECISION, preferred_element_type=jnp.float32
@@ -491,8 +342,10 @@
 STATE_ROWS = 8
 
 
-def mixer_kernel(
+def layer_kernel(
     chips,
+    cap,
+    chunks,
     narrow_in,
     wide_in,
     narrow_gate,
@@ -511,8 +364,13 @@
     resid_hbm,
     narrow_rows_hbm,
     wide_rows_hbm,
-    normed_out,
-    state_out,
+    routes,
+    routes_turned,
+    weights,
+    gate_hbm,
+    up_hbm,
+    down_hbm,
+    out,
     keys,
     queries,
     resid,
@@ -545,24 +403,34 @@
     sum_got,
     square_sent,
     square_got,
+    state,
+    choice,
+    share,
+    outgoing,
+    tokens,
+    gate_up,
+    down,
+    blocks,
+    line_relay,
+    line_sums,
+    result,
+    back,
+    weight_load,
+    weight_sent,
+    weight_got,
+    out_sent,
+    out_got,
+    line_sent,
+    line_got,
+    back_sent,
+    back_got,
 ):
     place = Place(chips)
     devices = chips * CORES
     length = narrow_in.shape[0]
     width = keys.shape[1]
     plane = SIDE * SIDE
-    barrier = pltpu.get_barrier_semaphore()
-    count = 0
-    for step in range(1, plane):
-        pl.semaphore_signal(
-            barrier, inc=1, device_id=(place.sp, (place.tp + step) % plane), device_id_type=MESH
-        )
-        count += 1
-    for step in range(1, devices):
-        pl.semaphore_signal(
-            barrier, inc=1, device_id=((place.sp + step) % devices, place.tp), device_id_type=MESH
-        )
-        count += 1
+    barrier, count = greet(place)
     group = pl.multiple_of((place.tp // (HEADS // GROUPS)) * width, width)
     mine = pl.ds(pl.multiple_of(place.tp * width, width), width)
     pairs = (
@@ -572,6 +440,8 @@
         (narrow_rows_hbm, narrow_rows),
         (wide_rows_hbm, wide_rows),
     )
+    gather = Gather(place, gate_up, down, weight_sent, weight_got)
+    gather.load(gate_hbm, up_hbm, down_hbm, weight_load)
     loads = [pltpu.make_async_copy(src, dst, load_sem.at[k]) for k, (src, dst) in enumerate(pairs)]
     for load in loads:
         load.start()
@@ -602,6 +472,7 @@
     loads[0].wait()
     loads[1].wait()
     pl.semaphore_wait(barrier, count)
+    gather.open()
     following = ((place.sp + 1) % devices, place.tp)
     rims = []
     tail = pl.ds(length - RIM, RIM)
@@ -677,6 +548,7 @@
 
     for copy in tells:
         copy.wait_recv()
+    gather.pass_on(0)
     running = jnp.zeros((STATE_ROWS, width), jnp.float32)
     upper_rows = iota((STATE_ROWS, width), 0) < per
     for source in range(devices):
@@ -688,11 +560,13 @@
         factor = jnp.exp(jnp.where(upper_rows, wide_total, narrow_total))
         running = factor * running + piece
     answers = exchange(answer, carried, answer_sent, answer_got)
+    routing_tables(devices, cap, routes, routes_turned, weights, choice, share)
 
     for load in loads[2:]:
         load.wait()
     for copy in answers:
         copy.wait_recv()
+    gather.pass_on(1)
     entering = carried[...].astype(jnp.float32).reshape(devices * STATE_ROWS, width)
 
     def head(inside, asked, size, kind, mix, opened, gain):
@@ -709,7 +583,7 @@
             place, first, partial.at[u], relay.at[u], sums.at[u], half.at[u], last.at[u],
             sum_sent.at[u], sum_got.at[u],
         )
-        for u, first in ((0, "x"), (1, "y"))
+        for u, first in ((0, "y"), (1, "y"))
     ]
     unit = length // 2
     for i in range(SIDE):
@@ -724,9 +598,9 @@
             getattr(total, move)()
     mixed = jnp.concatenate([total.close() for total in totals_of], axis=0)
     hidden = resid[...].astype(jnp.float32) + mixed
-    state_out[...] = hidden
     ones = jnp.ones((8, width), jnp.float32)
     own = fine_dot(ones, hidden * hidden, (((1,), (1,)), ((), ())))[0:1, :]
+    gather.pass_on(2)
     squares_out[...] = own
     squares[place.tp] = own
     shares = []
@@ -745,9 +619,147 @@
         whole = whole + squares[k]
     diagonal = iota((length, length), 0) == iota((length, length), 1)
     mean = jnp.sum(jnp.where(diagonal, whole, 0.0), axis=1, keepdims=True) * (1.0 / (plane * width))
-    normed_out[...] = (
-        hidden * lax.rsqrt(mean + NORM_EPS) * last_gain[:, mine]
-    ).astype(jnp.bfloat16)
+    state[...] = hidden
+    normed = (hidden * lax.rsqrt(mean + NORM_EPS) * last_gain[:, mine]).astype(jnp.bfloat16)
+
+    outgoing[...] = dot(choice[...], normed).astype(jnp.bfloat16)
+    order = chip_order(chips)
+    spot = {d: k for k, d in enumerate(order)}
+    y, x, core = place.at["y"], place.at["x"], place.core
+    home = spot[0]
+    inside = x == 2 * (home % 2) + core
+    outside = x != 2 * (home % 2) + core
+    waits = []
+
+    def slot_rows(number):
+        return pl.ds(pl.multiple_of(number * cap, cap), cap)
+
+    def guarded(apart, act):
+        if apart:
+            pl.when(outside)(act)
+        else:
+            act()
+
+    for s, d in enumerate(order):
+        for other in (0, 1):
+            aim = core if other == 0 else 1 - core
+            target = ((place.z + chips - d) % chips) * CORES + aim
+            device = (target, y * SIDE + 2 * (s % 2) + core)
+            rows = slot_rows(target)
+            to = pl.ds((s // 2) * cap, cap)
+            copy = remote(
+                outgoing.at[rows],
+                tokens.at[y, x, to],
+                out_sent.at[s * 2 + other],
+                out_got.at[s // 2, x],
+                device,
+            )
+            apart = d == 0 and other == 0
+            guarded(apart, copy.start)
+            waits.append((apart, copy))
+            if apart:
+
+                @pl.when(inside)
+                def _(rows=rows, to=to):
+                    tokens[y, x, to, :] = outgoing[rows, :]
+
+    units = chips // 2
+    per = units // chunks
+    size = per * cap
+    parts = []
+
+    def steps(k):
+        rows = pl.ds(k * size, size)
+        line = Line(
+            place, tokens.at[:, :, rows], blocks.at[k], line_relay.at[k], line_sums.at[k],
+            line_sent.at[k], line_got.at[k],
+        )
+        parts.append(line)
+
+        def arrive():
+            for u in range(k * per, (k + 1) * per):
+                for side in range(SIDE):
+                    column = (x + side) % SIDE
+                    to = pl.ds(u * cap, cap)
+                    copy = remote(
+                        outgoing.at[pl.ds(0, cap)],
+                        tokens.at[y, column, to],
+                        out_sent.at[0],
+                        out_got.at[u, column],
+                        place.plane("y", 1),
+                    )
+                    guarded(side == 0 and u == home // 2, copy.wait_recv)
+            line.open()
+
+        def compute():
+            line.arrived()
+            if k == 0:
+                gather.close()
+            values = jnp.concatenate(
+                [tokens[i, j, rows, :] for i in range(SIDE) for j in range(SIDE)], axis=1
+            )
+            both = dot(values, gate_up[...])
+            hidden_units = both.shape[1] // 2
+            gate = jnp.minimum(both[:, :hidden_units], CLAMP_LIMIT)
+            up = jnp.clip(both[:, hidden_units:], -CLAMP_LIMIT, CLAMP_LIMIT)
+            act = ((up + 1.0) * gate * jax.nn.sigmoid(SIGMOID_SCALE * gate)).astype(jnp.bfloat16)
+            for i in range(SIDE):
+                wide_part = dot(act, down[:, i * SIDE * width : (i + 1) * SIDE * width])
+                for j in range(SIDE):
+                    blocks[k, i, j] = wide_part[:, j * width : (j + 1) * width].astype(jnp.bfloat16)
+            line.give()
+
+        def close():
+            result[k] = line.total().astype(jnp.bfloat16)
+            for u in range(k * per, (k + 1) * per):
+                d = order[2 * u] + (x // 2) * (order[2 * u + 1] - order[2 * u])
+                source = ((place.z + d) % chips) * CORES + x % 2
+                number = (2 * u + x // 2) * 2 + (x % 2 + core) % 2
+                piece = pl.ds((u - k * per) * cap, cap)
+                for side in range(SIDE):
+                    column = (x + side) % SIDE
+                    copy = remote(
+                        result.at[k, column, piece],
+                        back.at[slot_rows(place.sp)],
+                        back_sent.at[u, side],
+                        back_got.at[number],
+                        (source, y * SIDE + column),
+                    )
+                    apart = side == 0 and u == home // 2
+                    guarded(apart, copy.start)
+                    waits.append((apart, copy))
+                    if apart:
+
+                        @pl.when(inside)
+                        def _(piece=piece):
+                            back[slot_rows(place.sp), :] = result[k, x, piece, :]
+
+        return [arrive, line.pass_on, compute, line.add, close]
+
+    plans = [steps(k) for k in range(chunks)]
+    depth = len(plans[0])
+    turns = sorted((k + LAG * n, -n, k) for k in range(chunks) for n in range(depth))
+    for _, n, k in turns:
+        plans[k][-n]()
+    for s in range(chips):
+        for other in (0, 1):
+            copy = remote(
+                outgoing.at[pl.ds(0, cap)],
+                back.at[pl.ds(0, cap)],
+                out_sent.at[0],
+                back_got.at[s * 2 + other],
+                place.plane("y", 1),
+            )
+            guarded(s == home and other == 0, copy.wait_recv)
+    combined = state[...] + dot(share[0], back[...]) + dot(share[1], back[...])
+    out[...] = combined.astype(jnp.bfloat16)
+    for apart, copy in waits:
+        guarded(apart, copy.wait_send)
+    for copy in gather.started.values():
+        copy.wait_send()
+    for line in parts:
+        for copy in line.started:
+            copy.wait_send()
     for copy in rims + tells + answers + shares:
         copy.wait_send()
     for total in totals_of:
@@ -755,41 +767,28 @@
             copy.wait_send()
 
 
-def mixer_layer(
-    narrow_in,
-    wide_in,
-    narrow_gate,
-    wide_gate,
-    columns,
-    narrow_taps,
-    wide_taps,
-    key_taps,
-    query_taps,
-    narrow_gain,
-    wide_gain,
-    last_gain,
-    key_in,
-    query_in,
-    resid,
-    narrow_rows,
-    wide_rows,
-    chips,
+def layer_call(
+    inputs, loose, chips, cap
 ):
-    length, width = wide_in.shape
+    length, width = inputs[1].shape
+    narrow_in = inputs[0]
+    narrow_rows, wide_rows, gate_hbm, down_hbm = loose[3], loose[4], loose[5], loose[7]
     devices = chips * CORES
     plane = SIDE * SIDE
     unit = length // 2
+    chunks = CHUNKS
+    slots = devices * cap
+    rows = slots // SIDE
+    size = rows // chunks
+    features, hidden_units = gate_hbm.shape
     bf16, f32 = jnp.bfloat16, jnp.float32
     vmem, any_ = pl.BlockSpec(memory_space=pltpu.VMEM), pl.BlockSpec(memory_space=pl.ANY)
     dma = pltpu.SemaphoreType.DMA
     return pl.pallas_call(
-        functools.partial(mixer_kernel, chips),
-        out_shape=(
-            jax.ShapeDtypeStruct((length, width), bf16),
-            jax.ShapeDtypeStruct((length, width), f32),
-        ),
-        in_specs=[vmem] * 13 + [any_] * 5,
-        out_specs=(vmem, vmem),
+        functools.partial(layer_kernel, chips, cap, chunks),
+        out_shape=jax.ShapeDtypeStruct((length, width), bf16),
+        in_specs=[vmem] * 13 + [any_] * 5 + [vmem] * 3 + [any_] * 3,
+        out_specs=vmem,
         scratch_shapes=[
             pltpu.VMEM((length, width), bf16),
             pltpu.VMEM((length, width), bf16),
@@ -823,30 +822,36 @@
             dma((2, 8)),
             dma((plane,)),
             dma((plane,)),
+            pltpu.VMEM((length, width), f32),
+            pltpu.VMEM((slots, length), bf16),
+            pltpu.VMEM((2, length, slots), bf16),
+            pltpu.VMEM((slots, width), bf16),
+            pltpu.VMEM((SIDE, SIDE, rows, width), bf16),
+            pltpu.VMEM((features, 2 * SIDE * hidden_units), bf16),
+            pltpu.VMEM((SIDE * hidden_units, features), bf16),
+            pltpu.VMEM((chunks, SIDE, SIDE, size, width), bf16),
+            pltpu.VMEM((chunks, 2, SIDE, size // 2, width), bf16),
+            pltpu.VMEM((chunks, 2, SIDE, size, width), bf16),
+            pltpu.VMEM((chunks, SIDE, size, width), bf16),
+            pltpu.VMEM((slots, width), bf16),
+            dma((3,)),
+            dma((3, 4)),
+            dma((3, 4)),
+            dma((devices,)),
+            dma((chips // 2, SIDE)),
+            dma((chunks, 8)),
+            dma((chunks, 8)),
+            dma((chips // 2, SIDE)),
+            dma((devices,)),
         ],
         compiler_params=pltpu.CompilerParams(
             collective_id=0, has_side_effects=True, vmem_limit_bytes=56 * 1024 * 1024
         ),
-    )(
-        narrow_in,
-        wide_in,
-        narrow_gate,
-        wide_gate,
-        columns,
-        columns.T,
-        narrow_taps,
-        wide_taps,
-        key_taps,
-        query_taps,
-        narrow_gain.reshape(1, -1),
-        wide_gain.reshape(1, -1),
-        last_gain.reshape(1, -1),
-        key_in,
-        query_in,
-        resid,
-        narrow_rows,
-        wide_rows,
-    )
+    )(*inputs, *loose[:5], *inputs_of_routes(loose), *loose[5:8])
+
+
+def inputs_of_routes(loose):
+    return loose[8], loose[8].T, loose[9]
 
 
 def local(
@@ -881,37 +886,35 @@
     decays = -jnp.exp(head_decay_logarithm[:, 0])[None, :] * steps + position_log_decay[:, :, 0]
     direct = jnp.broadcast_to(direct_input_weight[:, 0][None, :], steps.shape)
     columns = jnp.concatenate([steps, decays, direct, jnp.zeros_like(direct)], axis=1)
-    own_columns, own_state = mixer_layer(
+    length, picks = routes.shape
+    inputs = (
         narrow_head_input,
         wide_head_input,
         narrow_output_gate,
         wide_output_gate,
         columns,
+        columns.T,
         narrow_conv_taps,
         wide_conv_taps,
         key_conv_taps,
         query_conv_taps,
-        narrow_norm_gain,
-        wide_norm_gain,
-        feedforward_norm_gain,
+        narrow_norm_gain.reshape(1, -1),
+        wide_norm_gain.reshape(1, -1),
+        feedforward_norm_gain.reshape(1, -1),
+    )
+    loose = (
         key_group_input,
         query_group_input,
         resid,
         narrow_output_rows,
         wide_output_rows,
-        chips,
-    )
-    return expert_layer(
-        own_columns,
-        own_state,
-        routes,
-        routing_weight_values,
         expert_gate_matrix[0],
         expert_up_matrix[0],
         expert_down_matrix[0],
-        chips,
-        2,
+        routes,
+        routing_weight_values,
     )
+    return layer_call(inputs, loose, chips, 4 * length * picks // (3 * chips * CORES))
 
 
 def solution(mesh):

time: 156 us -> 139 us (0.89); the launches traced: 154 us -> 139 us
  Pallas kernels: 146 us -> 131 us
    pallas_call x2 -> x1, Pallas kernels: 146 us -> 131 us  [layer_call(): pl.pallas_call(functools.partial(layer_kernel, chips, cap, chunks), out_s...]
where the time goes in v3:
time: 139 us
  Pallas kernels  131 us (94%)
  local copies, waits for them, and re-layouts  6.05 us (4%)
  other arithmetic  2.09 us (2%)
    pallas_call x1, Pallas kernels, layer_call(): pl.pallas_call(functools.partial(layer_kernel, chips, cap, chunks), out_s...  131 us
    unnamed x13, local copies, waits for them, and re-layouts  4.54 us

profile of v3, /device:TPU:6, one launch (start us, length us, event | category | flops | bytes accessed | tf_op | source)
XLA Modules:
  0.0 138.9 jit_solution(16533794539216730096)
XLA Ops:
  0.0 0.0 copy-start
  0.0 0.7 negate_bitcast_fusion
  0.7 0.7 pad.2.clone
  1.4 0.8 compare_select_fusion
  2.2 0.7 fusion.4
  2.8 0.0 copy-done
  2.8 0.0 copy-start.1
  2.8 0.7 copy.26.narrow_in
  3.6 0.0 copy-done.1
  3.6 0.7 copy.27.narrow_gate
  4.3 0.0 copy-start.3
  4.3 0.8 copy.28.columns
  5.1 0.0 copy-done.3
  5.1 0.0 copy-start.2
  5.1 0.8 copy.30.weights
  5.9 0.0 copy-done.2
  5.9 0.8 copy.29.routes
  6.7 130.7 %shard_map.235 = bf16[256,128]{1,0:T(8,128)(2,1)} custom-call(bf16[256,64]{1,0:T(8,128)(2,1)} %copy.26.narrow_in, bf16[256,128]{1,0:T(8,128)(2,1)} %wide_in.1, bf16[256,64]{1,0:T(8,128)(2,1)} %copy.27.narrow_gate, bf16[256,128]{1,0:T(8,128)(2,1)} %wide_gate.1, f32[256,8]{1,0:T(8,128)} %copy.28.columns, f32[8,256]{1,0:T(8,128)} %get-tuple-element.5.lines, ...), custom_call_target="tpu_custom_call" | custom-call | tf_op jit(solution)/shard_map/pallas_call | solution.py:787
  137.4 1.5 %copy.34 = bf16[256,128]{1,0:T(8,128)(2,1)} copy(bf16[256,128]{1,0:T(8,128)(2,1)} %shard_map.235) | data formatting | bytes 131072
  (1 shorter events, 0.0 us)
Async XLA Ops:
  0.0 2.8 %copy-start = (bf16[256,64]{0,1:T(8,128)(2,1)S(1)}, bf16[256,64]{0,1:T(8,128)(2,1)}, u32[]{:S(2)}) copy-start(bf16[256,64]{0,1:T(8,128)(2,1)} %param.26) | copy-start | bytes 98308
  2.8 0.8 copy-start.1
  4.3 0.8 copy-start.3
  5.1 0.8 copy-start.2

commit v4 on v3

--- a/solution.py
+++ b/solution.py
@@ -47,7 +47,20 @@
         self.z, self.core = self.sp // CORES, self.sp % CORES
         self.at = {"y": self.tp // SIDE, "x": self.tp % SIDE}
 
+        self.at["a"] = self.pick(self.core, self.at["x"], self.at["y"])
+        self.at["b"] = self.pick(self.core, self.at["y"], self.at["x"])
+
+    def pick(self, core, first, second):
+        return first + core * (second - first)
+
+    def flat(self, core, a, b):
+        return b * (SIDE - (SIDE - 1) * core) + a * (1 + (SIDE - 1) * core)
+
     def plane(self, axis, step):
+        if axis == "a":
+            return (self.sp, self.flat(self.core, self.index("a", step), self.at["b"]))
+        if axis == "b":
+            return (self.sp, self.flat(self.core, self.at["a"], self.index("b", step)))
         moved = (self.at[axis] + step + SIDE) % SIDE
         if axis == "x":
             return (self.sp, self.at["y"] * SIDE + moved)
@@ -70,19 +83,24 @@
     barrier = pltpu.get_barrier_semaphore()
     count = 0
     devices = place.chips * CORES
+
+    def tell(sp, a, b):
+        device = (sp, place.flat(place.core, a, b))
+        pl.semaphore_signal(barrier, inc=1, device_id=device, device_id_type=MESH)
+
+    own_a, own_b = place.at["a"], place.at["b"]
     for step in range(devices):
         for side in range(SIDE):
             if step or side:
-                device = (
-                    (place.sp + step) % devices,
-                    place.at["y"] * SIDE + (place.at["x"] + side) % SIDE,
-                )
-                pl.semaphore_signal(barrier, inc=1, device_id=device, device_id_type=MESH)
+                tell((place.sp + step) % devices, (own_a + side) % SIDE, own_b)
                 count += 1
-    for step in range(1, SIDE):
-        for side in range(SIDE):
-            device = (place.sp, ((place.at["y"] + step) % SIDE) * SIDE + (place.at["x"] + side) % SIDE)
-            pl.semaphore_signal(barrier, inc=1, device_id=device, device_id_type=MESH)
+    for side in range(1, SIDE):
+        for step in range(place.chips):
+            other = ((place.z + step) % place.chips) * CORES + 1 - place.core
+            tell(other, own_a, (own_b + side) % SIDE)
+            count += 1
+        for step in range(SIDE):
+            tell(place.sp, (own_a + step) % SIDE, (own_b + side) % SIDE)
             count += 1
     return barrier, count
 
@@ -94,7 +112,7 @@
         self.width = down.shape[0] // SIDE
 
     def piece(self, kind, step, part=None):
-        index = self.place.index("x", step)
+        index = self.place.index("a", step)
         if kind == 2:
             ref = self.down.at[pl.ds(pl.multiple_of(index * self.width, self.width), self.width)]
         else:
@@ -107,21 +125,38 @@
 
     def load(self, gate_hbm, up_hbm, down_hbm, sem):
         for kind, src in enumerate((gate_hbm, up_hbm, down_hbm)):
-            copy = pltpu.make_async_copy(src, self.piece(kind, 0), sem.at[kind])
-            copy.start()
-            self.loads.append(copy)
+            dst = self.piece(kind, 0)
+            copies = []
+            for i in range(SIDE):
+                for j in range(SIDE):
+                    number = i * SIDE + j
+                    there = self.place.flat(self.place.core, j, i) * self.width
+                    there = pl.ds(pl.multiple_of(there, self.width), self.width)
+                    here = pl.ds(number * self.width, self.width)
+                    if kind == 2:
+                        copy = pltpu.make_async_copy(
+                            src.at[:, there], dst.at[:, here], sem.at[kind, number]
+                        )
+                    else:
+                        copy = pltpu.make_async_copy(
+                            src.at[there], dst.at[here], sem.at[kind, number]
+                        )
+                    copy.start()
+                    copies.append(copy)
+            self.loads.append(copies)
 
     def send(self, ref, kind, number, step):
         copy = remote(
             ref, ref, self.sent.at[kind, number], self.got.at[kind, number],
-            self.place.plane("x", step),
+            self.place.plane("a", step),
         )
         copy.start()
         self.started[(kind, number)] = copy
 
     def open(self):
         for kind in range(3):
-            self.loads[kind].wait()
+            for copy in self.loads[kind]:
+                copy.wait()
             self.send(self.piece(kind, 0), kind, 0, 1)
             self.send(self.piece(kind, 0), kind, 1, SIDE - 1)
 
@@ -148,13 +183,13 @@
     def send(self, src, dst, step):
         number = len(self.started)
         copy = remote(
-            src, dst, self.sent.at[number], self.got.at[number], self.place.plane("y", step)
+            src, dst, self.sent.at[number], self.got.at[number], self.place.plane("b", step)
         )
         copy.start()
         self.started.append(copy)
 
     def open(self):
-        own = self.tokens.at[self.place.at["y"]]
+        own = self.tokens.at[self.place.at["b"]]
         self.send(own, own, 1)
         self.send(own, own, SIDE - 1)
 
@@ -162,7 +197,7 @@
         for side, step in ((0, SIDE - 1), (1, 1)):
             self.started[side].wait_recv()
             part = self.low if side == 0 else self.high
-            ref = self.tokens.at[self.place.index("y", step)].at[:, part]
+            ref = self.tokens.at[self.place.index("b", step)].at[:, part]
             self.send(ref, ref, SIDE - step)
 
     def arrived(self):
@@ -170,7 +205,7 @@
         self.started[3].wait_recv()
 
     def give(self):
-        far = self.blocks.at[self.place.index("y", 2)]
+        far = self.blocks.at[self.place.index("b", 2)]
         self.send(far.at[:, self.low], self.relay.at[0], 1)
         self.send(far.at[:, self.high], self.relay.at[1], SIDE - 1)
 
@@ -178,7 +213,7 @@
         for side, step in ((0, 1), (1, SIDE - 1)):
             part = self.low if side == 0 else self.high
             self.started[4 + side].wait_recv()
-            near = self.blocks.at[self.place.index("y", step)]
+            near = self.blocks.at[self.place.index("b", step)]
             piece = near.at[:, part]
             piece[...] = (
                 piece[...].astype(jnp.float32) + self.relay[side].astype(jnp.float32)
@@ -189,7 +224,7 @@
         self.started[6].wait_recv()
         self.started[7].wait_recv()
         return (
-            self.blocks[self.place.at["y"]].astype(jnp.float32)
+            self.blocks[self.place.at["b"]].astype(jnp.float32)
             + self.sums[0].astype(jnp.float32)
             + self.sums[1].astype(jnp.float32)
         )
@@ -324,6 +359,11 @@
     return lax.dot_general(
         a, b, dims, precision=FULL_PRECISION, preferred_element_type=jnp.float32
     )
+
+
+def quick_dot(a, b, dims=(((1,), (0,)), ((), ()))):
+    a, b = a.astype(jnp.bfloat16), b.astype(jnp.bfloat16)
+    return lax.dot_general(a, b, dims, preferred_element_type=jnp.float32)
 
 
 def in_three(x):
@@ -506,10 +546,10 @@
     narrow_value, wide_value = narrow_mix * steps[0], wide_mix * steps[1]
 
     turned = (((0,), (0,)), ((), ()))
-    wide_keys = fine_dot(key, wide_spread)
-    narrow_keys = fine_dot(key, narrow_spread)
-    wide_state = fine_dot(wide_keys, wide_value * tails[1], turned)
-    narrow_state = fine_dot(
+    wide_keys = quick_dot(key, wide_spread)
+    narrow_keys = quick_dot(key, narrow_spread)
+    wide_state = quick_dot(wide_keys, wide_value * tails[1], turned)
+    narrow_state = quick_dot(
         narrow_keys,
         jnp.concatenate(
             [narrow_value * tails[0], jnp.zeros((length, width - narrow_size), jnp.float32)], axis=1
@@ -537,11 +577,11 @@
 
     tells = exchange(told, heard, told_sent, told_got)
 
-    scores = fine_dot(query, key, (((1,), (1,)), ((), ())))
-    narrow_inside = fine_dot(scores * decay[0], narrow_value)
-    wide_inside = fine_dot(scores * decay[1], wide_value)
-    wide_query = fine_dot(query * fades[1], wide_spread)
-    narrow_query = fine_dot(query * fades[0], narrow_spread)
+    scores = quick_dot(query, key, (((1,), (1,)), ((), ())))
+    narrow_inside = quick_dot(scores * decay[0], narrow_value)
+    wide_inside = quick_dot(scores * decay[1], wide_value)
+    wide_query = quick_dot(query * fades[1], wide_spread)
+    narrow_query = quick_dot(query * fades[0], narrow_spread)
     narrow_open, wide_open = silu(narrow_gate[...].astype(jnp.float32)), silu(
         wide_gate[...].astype(jnp.float32)
     )
@@ -570,7 +610,7 @@
     entering = carried[...].astype(jnp.float32).reshape(devices * STATE_ROWS, width)
 
     def head(inside, asked, size, kind, mix, opened, gain):
-        result = inside + fine_dot(asked, entering)[:, :size]
+        result = inside + quick_dot(asked, entering)[:, :size]
         result = (result + tall[:, 4 + kind : 5 + kind] * mix) * opened
         mean = jnp.sum(result * result, axis=-1, keepdims=True) * (1.0 / size)
         return (result * lax.rsqrt(mean + NORM_EPS) * gain[...]).astype(jnp.bfloat16)
@@ -583,7 +623,7 @@
             place, first, partial.at[u], relay.at[u], sums.at[u], half.at[u], last.at[u],
             sum_sent.at[u], sum_got.at[u],
         )
-        for u, first in ((0, "y"), (1, "y"))
+        for u, first in ((0, "x"), (1, "y"))
     ]
     unit = length // 2
     for i in range(SIDE):
@@ -625,10 +665,10 @@
     outgoing[...] = dot(choice[...], normed).astype(jnp.bfloat16)
     order = chip_order(chips)
     spot = {d: k for k, d in enumerate(order)}
-    y, x, core = place.at["y"], place.at["x"], place.core
+    row, column_own, core = place.at["b"], place.at["a"], place.core
     home = spot[0]
-    inside = x == 2 * (home % 2) + core
-    outside = x != 2 * (home % 2) + core
+    inside = column_own == 2 * (home % 2) + core
+    outside = column_own != 2 * (home % 2) + core
     waits = []
 
     def slot_rows(number):
@@ -644,14 +684,16 @@
         for other in (0, 1):
             aim = core if other == 0 else 1 - core
             target = ((place.z + chips - d) % chips) * CORES + aim
-            device = (target, y * SIDE + 2 * (s % 2) + core)
+            across = place.pick(aim, place.at["x"], place.at["y"])
+            along = place.pick(aim, place.at["y"], place.at["x"])
+            device = (target, place.flat(aim, 2 * (s % 2) + core, along))
             rows = slot_rows(target)
             to = pl.ds((s // 2) * cap, cap)
             copy = remote(
                 outgoing.at[rows],
-                tokens.at[y, x, to],
+                tokens.at[along, across, to],
                 out_sent.at[s * 2 + other],
-                out_got.at[s // 2, x],
+                out_got.at[s // 2, across],
                 device,
             )
             apart = d == 0 and other == 0
@@ -661,7 +703,7 @@
 
                 @pl.when(inside)
                 def _(rows=rows, to=to):
-                    tokens[y, x, to, :] = outgoing[rows, :]
+                    tokens[row, column_own, to, :] = outgoing[rows, :]
 
     units = chips // 2
     per = units // chunks
@@ -679,14 +721,14 @@
         def arrive():
             for u in range(k * per, (k + 1) * per):
                 for side in range(SIDE):
-                    column = (x + side) % SIDE
+                    column = (column_own + side) % SIDE
                     to = pl.ds(u * cap, cap)
                     copy = remote(
                         outgoing.at[pl.ds(0, cap)],
-                        tokens.at[y, column, to],
+                        tokens.at[row, column, to],
                         out_sent.at[0],
                         out_got.at[u, column],
-                        place.plane("y", 1),
+                        place.plane("b", 1),
                     )
                     guarded(side == 0 and u == home // 2, copy.wait_recv)
             line.open()
@@ -712,18 +754,18 @@
         def close():
             result[k] = line.total().astype(jnp.bfloat16)
             for u in range(k * per, (k + 1) * per):
-                d = order[2 * u] + (x // 2) * (order[2 * u + 1] - order[2 * u])
-                source = ((place.z + d) % chips) * CORES + x % 2
-                number = (2 * u + x // 2) * 2 + (x % 2 + core) % 2
+                d = order[2 * u] + (column_own // 2) * (order[2 * u + 1] - order[2 * u])
+                source = ((place.z + d) % chips) * CORES + column_own % 2
+                number = (2 * u + column_own // 2) * 2 + (column_own % 2 + core) % 2
                 piece = pl.ds((u - k * per) * cap, cap)
                 for side in range(SIDE):
-                    column = (x + side) % SIDE
+                    column = (column_own + side) % SIDE
                     copy = remote(
                         result.at[k, column, piece],
                         back.at[slot_rows(place.sp)],
                         back_sent.at[u, side],
                         back_got.at[number],
-                        (source, y * SIDE + column),
+                        (source, place.flat(core, column, row)),
                     )
                     apart = side == 0 and u == home // 2
                     guarded(apart, copy.start)
@@ -732,7 +774,7 @@
 
                         @pl.when(inside)
                         def _(piece=piece):
-                            back[slot_rows(place.sp), :] = result[k, x, piece, :]
+                            back[slot_rows(place.sp), :] = result[k, column_own, piece, :]
 
         return [arrive, line.pass_on, compute, line.add, close]
 
@@ -748,7 +790,7 @@
                 back.at[pl.ds(0, cap)],
                 out_sent.at[0],
                 back_got.at[s * 2 + other],
-                place.plane("y", 1),
+                place.plane("b", 1),
             )
             guarded(s == home and other == 0, copy.wait_recv)
     combined = state[...] + dot(share[0], back[...]) + dot(share[1], back[...])
@@ -834,7 +876,7 @@
             pltpu.VMEM((chunks, 2, SIDE, size, width), bf16),
             pltpu.VMEM((chunks, SIDE, size, width), bf16),
             pltpu.VMEM((slots, width), bf16),
-            dma((3,)),
+            dma((3, SIDE * SIDE)),
             dma((3, 4)),
             dma((3, 4)),
             dma((devices,)),

time: 139 us -> 124 us (0.89)
  Pallas kernels: 131 us -> 115 us
    pallas_call x1, Pallas kernels: 131 us -> 115 us  [layer_call(): pl.pallas_call(functools.partial(layer_kernel, chips, cap, chunks), out_s...]
where the time goes in v4:
time: 124 us; the launch traced here: 123 us
  Pallas kernels  115 us (93%)
  local copies, waits for them, and re-layouts  6.05 us (5%)
  other arithmetic  2.09 us (2%)
    pallas_call x1, Pallas kernels, layer_call(): pl.pallas_call(functools.partial(layer_kernel, chips, cap, chunks), out_s...  115 us
    unnamed x13, local copies, waits for them, and re-layouts  4.54 us

profile of v4, /device:TPU:6, one launch (start us, length us, event | category | flops | bytes accessed | tf_op | source)
XLA Modules:
  0.0 123.3 jit_solution(2779095032797229045)
XLA Ops:
  0.0 0.0 copy-start
  0.0 0.7 negate_bitcast_fusion
  0.7 0.7 pad.2.clone
  1.4 0.8 compare_select_fusion
  2.2 0.7 fusion.4
  2.8 0.0 copy-done
  2.8 0.0 copy-start.1
  2.8 0.7 copy.26.narrow_in
  3.6 0.0 copy-done.1
  3.6 0.7 copy.27.narrow_gate
  4.3 0.0 copy-start.3
  4.3 0.8 copy.28.columns
  5.1 0.0 copy-done.3
  5.1 0.0 copy-start.2
  5.1 0.8 copy.30.weights
  5.9 0.0 copy-done.2
  5.9 0.8 copy.29.routes
  6.7 115.2 %shard_map.235 = bf16[256,128]{1,0:T(8,128)(2,1)} custom-call(bf16[256,64]{1,0:T(8,128)(2,1)} %copy.26.narrow_in, bf16[256,128]{1,0:T(8,128)(2,1)} %wide_in.1, bf16[256,64]{1,0:T(8,128)(2,1)} %copy.27.narrow_gate, bf16[256,128]{1,0:T(8,128)(2,1)} %wide_gate.1, f32[256,8]{1,0:T(8,128)} %copy.28.columns, f32[8,256]{1,0:T(8,128)} %get-tuple-element.5.lines, ...), custom_call_target="tpu_custom_call" | custom-call | tf_op jit(solution)/shard_map/pallas_call | solution.py:829
  121.9 1.5 %copy.34 = bf16[256,128]{1,0:T(8,128)(2,1)} copy(bf16[256,128]{1,0:T(8,128)(2,1)} %shard_map.235) | data formatting | bytes 131072
  (1 shorter events, 0.0 us)
Async XLA Ops:
  0.0 2.8 %copy-start = (bf16[256,64]{0,1:T(8,128)(2,1)S(1)}, bf16[256,64]{0,1:T(8,128)(2,1)}, u32[]{:S(2)}) copy-start(bf16[256,64]{0,1:T(8,128)(2,1)} %param.26) | copy-start | bytes 98308
  2.8 0.8 copy-start.1
  4.3 0.8 copy-start.3
  5.1 0.8 copy-start.2

commit v5 on v4

--- a/solution.py
+++ b/solution.py
@@ -26,6 +26,7 @@
 SIDE = 4
 LAG = 2
 CHUNKS = 4
+PICKS = 3
 
 
 def remote(src, dst, send_sem, recv_sem, device):
@@ -99,9 +100,8 @@
             other = ((place.z + step) % place.chips) * CORES + 1 - place.core
             tell(other, own_a, (own_b + side) % SIDE)
             count += 1
-        for step in range(SIDE):
-            tell(place.sp, (own_a + step) % SIDE, (own_b + side) % SIDE)
-            count += 1
+        tell(place.sp, own_a, (own_b + side) % SIDE)
+        count += 1
     return barrier, count
 
 
@@ -320,13 +320,14 @@
     return high, (x - high.astype(jnp.float32)).astype(jnp.bfloat16)
 
 
-def routing_tables(experts, cap, routes, routes_turned, weights, choice, share):
-    tokens, picks = routes.shape
+def routing_tables(experts, cap, tall, flat, choice, share):
+    tokens, picks = tall.shape[0], PICKS
     slots = experts * cap
     shift = cap.bit_length() - 1
-    named = routes[...]
-    turned = routes_turned[...]
-    amount = weights[...]
+    start = 8 + picks
+    named = (tall[:, start : start + picks] + 0.5).astype(jnp.int32)
+    turned = (flat[start : start + picks, :] + 0.5).astype(jnp.int32)
+    amount = tall[:, 8 : 8 + picks]
     lines = iota((experts, tokens), 0)
     there = turned[0:1, :] == lines
     for k in range(1, picks):
@@ -386,11 +387,10 @@
     chips,
     cap,
     chunks,
-    narrow_in,
+    narrow_turned,
     wide_in,
-    narrow_gate,
+    gate_turned,
     wide_gate,
-    columns,
     lines,
     narrow_taps,
     wide_taps,
@@ -404,13 +404,11 @@
     resid_hbm,
     narrow_rows_hbm,
     wide_rows_hbm,
-    routes,
-    routes_turned,
-    weights,
     gate_hbm,
     up_hbm,
     down_hbm,
     out,
+    narrow_in,
     keys,
     queries,
     resid,
@@ -430,8 +428,6 @@
     sums,
     half,
     last,
-    squares_out,
-    squares,
     load_sem,
     rim_sent,
     rim_got,
@@ -441,8 +437,6 @@
     answer_got,
     sum_sent,
     sum_got,
-    square_sent,
-    square_got,
     state,
     choice,
     share,
@@ -489,7 +483,13 @@
     upper = ones_where(iota((length, length), 0) <= iota((length, length), 1))
     causal = iota((length, length), 0) >= iota((length, length), 1)
     lower = ones_where(causal)
-    tall, flat = columns[...], lines[...]
+    same = iota((length, length), 0) == iota((length, length), 1)
+    across = (((1,), (1,)), ((), ()))
+    flat = lines[...]
+    tall = fine_dot(jnp.where(same, 1.0, 0.0), flat, across)
+    narrow_in[...] = quick_dot(ones_where(same), narrow_turned[...], across).astype(jnp.bfloat16)
+    narrow_open = silu(quick_dot(ones_where(same), gate_turned[...], across))
+    wide_open = silu(wide_gate[...].astype(jnp.float32))
     tall_sum = sum(dot(lower, piece) for piece in in_three(tall))
     flat_sum = sum(dot(piece, upper) for piece in in_three(flat))
     decay, tails, totals, steps = [], [], [], []
@@ -582,9 +582,6 @@
     wide_inside = quick_dot(scores * decay[1], wide_value)
     wide_query = quick_dot(query * fades[1], wide_spread)
     narrow_query = quick_dot(query * fades[0], narrow_spread)
-    narrow_open, wide_open = silu(narrow_gate[...].astype(jnp.float32)), silu(
-        wide_gate[...].astype(jnp.float32)
-    )
 
     for copy in tells:
         copy.wait_recv()
@@ -600,7 +597,7 @@
         factor = jnp.exp(jnp.where(upper_rows, wide_total, narrow_total))
         running = factor * running + piece
     answers = exchange(answer, carried, answer_sent, answer_got)
-    routing_tables(devices, cap, routes, routes_turned, weights, choice, share)
+    routing_tables(devices, cap, tall, flat, choice, share)
 
     for load in loads[2:]:
         load.wait()
@@ -638,31 +635,9 @@
             getattr(total, move)()
     mixed = jnp.concatenate([total.close() for total in totals_of], axis=0)
     hidden = resid[...].astype(jnp.float32) + mixed
-    ones = jnp.ones((8, width), jnp.float32)
-    own = fine_dot(ones, hidden * hidden, (((1,), (1,)), ((), ())))[0:1, :]
     gather.pass_on(2)
-    squares_out[...] = own
-    squares[place.tp] = own
-    shares = []
-    for step in range(1, plane):
-        other = (place.tp + step) % plane
-        copy = remote(
-            squares_out, squares.at[place.tp], square_sent.at[step], square_got.at[step],
-            (place.sp, other),
-        )
-        copy.start()
-        shares.append(copy)
-    for copy in shares:
-        copy.wait_recv()
-    whole = squares[0]
-    for k in range(1, plane):
-        whole = whole + squares[k]
-    diagonal = iota((length, length), 0) == iota((length, length), 1)
-    mean = jnp.sum(jnp.where(diagonal, whole, 0.0), axis=1, keepdims=True) * (1.0 / (plane * width))
     state[...] = hidden
-    normed = (hidden * lax.rsqrt(mean + NORM_EPS) * last_gain[:, mine]).astype(jnp.bfloat16)
-
-    outgoing[...] = dot(choice[...], normed).astype(jnp.bfloat16)
+    outgoing[...] = dot(choice[...], hidden.astype(jnp.bfloat16)).astype(jnp.bfloat16)
     order = chip_order(chips)
     spot = {d: k for k, d in enumerate(order)}
     row, column_own, core = place.at["b"], place.at["a"], place.core
@@ -737,8 +712,20 @@
             line.arrived()
             if k == 0:
                 gather.close()
+            pairs_of = [(i, j) for i in range(SIDE) for j in range(SIDE)]
+            pieces = [tokens[i, j, rows, :].astype(jnp.float32) for i, j in pairs_of]
+            squared = sum(piece * piece for piece in pieces)
+            mean = jnp.sum(squared, axis=-1, keepdims=True) * (1.0 / (plane * width))
+            scale = lax.rsqrt(mean + NORM_EPS)
+            gains = [
+                last_gain[
+                    :, pl.ds(pl.multiple_of(place.flat(core, j, i) * width, width), width)
+                ]
+                for i, j in pairs_of
+            ]
             values = jnp.concatenate(
-                [tokens[i, j, rows, :] for i in range(SIDE) for j in range(SIDE)], axis=1
+                [(piece * scale * gain).astype(jnp.bfloat16) for piece, gain in zip(pieces, gains)],
+                axis=1,
             )
             both = dot(values, gate_up[...])
             hidden_units = both.shape[1] // 2
@@ -802,7 +789,7 @@
     for line in parts:
         for copy in line.started:
             copy.wait_send()
-    for copy in rims + tells + answers + shares:
+    for copy in rims + tells + answers:
         copy.wait_send()
     for total in totals_of:
         for copy in total.started:
@@ -813,10 +800,9 @@
     inputs, loose, chips, cap
 ):
     length, width = inputs[1].shape
-    narrow_in = inputs[0]
+    narrow_size = inputs[0].shape[0]
     narrow_rows, wide_rows, gate_hbm, down_hbm = loose[3], loose[4], loose[5], loose[7]
     devices = chips * CORES
-    plane = SIDE * SIDE
     unit = length // 2
     chunks = CHUNKS
     slots = devices * cap
@@ -829,15 +815,16 @@
     return pl.pallas_call(
         functools.partial(layer_kernel, chips, cap, chunks),
         out_shape=jax.ShapeDtypeStruct((length, width), bf16),
-        in_specs=[vmem] * 13 + [any_] * 5 + [vmem] * 3 + [any_] * 3,
+        in_specs=[vmem] * 12 + [any_] * 8,
         out_specs=vmem,
         scratch_shapes=[
+            pltpu.VMEM((length, narrow_size), bf16),
             pltpu.VMEM((length, width), bf16),
             pltpu.VMEM((length, width), bf16),
             pltpu.VMEM((length, width), bf16),
             pltpu.VMEM(narrow_rows.shape, bf16),
             pltpu.VMEM(wide_rows.shape, bf16),
-            pltpu.VMEM((RIM, narrow_in.shape[1]), bf16),
+            pltpu.VMEM((RIM, narrow_size), bf16),
             pltpu.VMEM((RIM, width), bf16),
             pltpu.VMEM((RIM, width), bf16),
             pltpu.VMEM((RIM, width), bf16),
@@ -851,8 +838,6 @@
             pltpu.VMEM((2, 2, SIDE, unit, width), bf16),
             pltpu.VMEM((2, 2, unit // 2, width), bf16),
             pltpu.VMEM((2, 2, unit, width), bf16),
-            pltpu.VMEM((1, length), f32),
-            pltpu.VMEM((plane, 1, length), f32),
             dma((5,)),
             dma((4,)),
             dma((4,)),
@@ -862,8 +847,6 @@
             dma((devices,)),
             dma((2, 8)),
             dma((2, 8)),
-            dma((plane,)),
-            dma((plane,)),
             pltpu.VMEM((length, width), f32),
             pltpu.VMEM((slots, length), bf16),
             pltpu.VMEM((2, length, slots), bf16),
@@ -889,11 +872,7 @@
         compiler_params=pltpu.CompilerParams(
             collective_id=0, has_side_effects=True, vmem_limit_bytes=56 * 1024 * 1024
         ),
-    )(*inputs, *loose[:5], *inputs_of_routes(loose), *loose[5:8])
-
-
-def inputs_of_routes(loose):
-    return loose[8], loose[8].T, loose[9]
+    )(*inputs, *loose)
 
 
 def local(
@@ -924,18 +903,29 @@
     expert_down_matrix,
 ):
     chips = lax.axis_size(SP) // CORES
-    steps = jax.nn.softplus(step_input_rows[:, :, 0].astype(jnp.float32))
-    decays = -jnp.exp(head_decay_logarithm[:, 0])[None, :] * steps + position_log_decay[:, :, 0]
-    direct = jnp.broadcast_to(direct_input_weight[:, 0][None, :], steps.shape)
-    columns = jnp.concatenate([steps, decays, direct, jnp.zeros_like(direct)], axis=1)
+    steps = jax.nn.softplus(step_input_rows[:, :, 0].T.astype(jnp.float32))
+    decays = -jnp.exp(head_decay_logarithm) * steps + position_log_decay[:, :, 0].T
+    direct = jnp.broadcast_to(direct_input_weight, steps.shape)
+    blank = jnp.zeros((2, steps.shape[1]), jnp.float32)
+    lines = jnp.concatenate(
+        [
+            steps,
+            decays,
+            direct,
+            blank,
+            routing_weight_values.T,
+            routes.T.astype(jnp.float32),
+            blank,
+        ],
+        axis=0,
+    )
     length, picks = routes.shape
     inputs = (
-        narrow_head_input,
+        narrow_head_input.T,
         wide_head_input,
-        narrow_output_gate,
+        narrow_output_gate.T,
         wide_output_gate,
-        columns,
-        columns.T,
+        lines,
         narrow_conv_taps,
         wide_conv_taps,
         key_conv_taps,
@@ -953,8 +943,6 @@
         expert_gate_matrix[0],
         expert_up_matrix[0],
         expert_down_matrix[0],
-        routes,
-        routing_weight_values,
     )
     return layer_call(inputs, loose, chips, 4 * length * picks // (3 * chips * CORES))
 

time: 124 us -> 114 us (0.919)
  Pallas kernels: 115 us -> 108 us
  other arithmetic: 2.09 us -> 0.07 us
    pallas_call x1, Pallas kernels: 115 us -> 108 us  [layer_call(): pl.pallas_call(functools.partial(layer_kernel, chips, cap, chunks), out_s...]
where the time goes in v5:
time: 114 us
  Pallas kernels  108 us (95%)
  local copies, waits for them, and re-layouts  5.34 us (5%)
    pallas_call x1, Pallas kernels, layer_call(): pl.pallas_call(functools.partial(layer_kernel, chips, cap, chunks), out_s...  108 us
    unnamed x13, local copies, waits for them, and re-layouts  4.04 us

profile of v5, /device:TPU:6, one launch (start us, length us, event | category | flops | bytes accessed | tf_op | source)
XLA Modules:
  0.0 113.9 jit_solution(9662624389679941260)
XLA Ops:
  0.0 0.0 copy-start.5
  0.0 0.0 copy-start.4
  0.0 0.7 copy-done.5
  0.7 0.0 copy-start.2
  0.7 0.0 copy-done.4
  0.7 0.0 copy-start.3
  0.7 0.1 broadcast_in_dim.9
  0.8 0.6 copy-done.2
  1.3 0.0 copy-done.3
  1.4 0.0 copy-start.1
  1.4 0.1 bitcast_add_fusion
  1.4 0.6 copy-done.1
  2.0 0.0 copy-start
  2.0 0.7 copy-done
  2.7 1.2 %concatenate.3.lines = f32[16,256]{1,0:T(8,128)} concatenate(f32[2,256]{1,0:T(2,128)S(1)} %get-tuple-element.6, f32[2,256]{1,0:T(2,128)S(1)} %get-tuple-element.5, f32[2,256]{1,0:T(2,128)S(1)} %broadcast_in_dim.9, f32[2,256]{1,0:T(2,128)S(1)} %max.8, f32[3,256]{1,0:T(4,128)S(1)} %bitcast.51, f32[3,256]{1,0:T(4,128)S(1)} %convert_bitcast_fusion, f32[2,256]{1,0:T(2,128)S(1)} %max.8), dimensions={0} | concatenate | bytes 32768 | tf_op jit(solution)/shard_map/concatenate | solution.py:910
  4.0 108.5 %shard_map.235 = bf16[256,128]{1,0:T(8,128)(2,1)} custom-call(bf16[64,256]{1,0:T(8,128)(2,1)} %bitcast.48, bf16[256,128]{1,0:T(8,128)(2,1)} %wide_in.1, bf16[64,256]{1,0:T(8,128)(2,1)} %bitcast.49, bf16[256,128]{1,0:T(8,128)(2,1)} %wide_gate.1, f32[16,256]{1,0:T(8,128)} %concatenate.3.lines, f32[4,64]{1,0:T(4,128)} %narrow_taps.1, f32[4,128]{1,0:T(4,128)} %wide_taps.1, ...), custom_call_target="tpu_custom_call" | custom-call | tf_op jit(solution)/shard_map/pallas_call | solution.py:815
  112.4 1.5 %copy.29 = bf16[256,128]{1,0:T(8,128)(2,1)} copy(bf16[256,128]{1,0:T(8,128)(2,1)} %shard_map.235) | data formatting | bytes 131072
  (3 shorter events, 0.0 us)
Async XLA Ops:
  0.0 0.7 copy-start.5
  0.0 0.7 copy-start.4
  0.7 0.7 copy-start.2
  0.7 0.7 copy-start.3
  1.4 0.7 copy-start.1
  2.0 0.7 copy-start

commit v6 on v5

--- a/solution.py
+++ b/solution.py
@@ -24,7 +24,7 @@
 MESH = pl.DeviceIdType.MESH
 CORES = 2
 SIDE = 4
-LAG = 2
+LAG = 1
 CHUNKS = 4
 PICKS = 3
 

time: 114 us -> 114 us (level)
  no operation moved by 1% of the time
where the time goes in v6:
time: 114 us
  Pallas kernels  109 us (96%)
  local copies, waits for them, and re-layouts  5.34 us (5%)
    pallas_call x1, Pallas kernels, layer_call(): pl.pallas_call(functools.partial(layer_kernel, chips, cap, chunks), out_s...  109 us
    unnamed x13, local copies, waits for them, and re-layouts  4.04 us

profile of v6, /device:TPU:6, one launch (start us, length us, event | category | flops | bytes accessed | tf_op | source)
XLA Modules:
  0.0 114.1 jit_solution(6915845367305942972)
XLA Ops:
  0.0 0.0 copy-start.5
  0.0 0.0 copy-start.4
  0.0 0.7 copy-done.5
  0.7 0.0 copy-start.2
  0.7 0.0 copy-done.4
  0.7 0.0 copy-start.3
  0.7 0.1 broadcast_in_dim.9
  0.8 0.6 copy-done.2
  1.3 0.0 copy-done.3
  1.4 0.0 copy-start.1
  1.4 0.1 bitcast_add_fusion
  1.4 0.6 copy-done.1
  2.0 0.0 copy-start
  2.0 0.7 copy-done
  2.7 1.2 %concatenate.3.lines = f32[16,256]{1,0:T(8,128)} concatenate(f32[2,256]{1,0:T(2,128)S(1)} %get-tuple-element.6, f32[2,256]{1,0:T(2,128)S(1)} %get-tuple-element.5, f32[2,256]{1,0:T(2,128)S(1)} %broadcast_in_dim.9, f32[2,256]{1,0:T(2,128)S(1)} %max.8, f32[3,256]{1,0:T(4,128)S(1)} %bitcast.51, f32[3,256]{1,0:T(4,128)S(1)} %convert_bitcast_fusion, f32[2,256]{1,0:T(2,128)S(1)} %max.8), dimensions={0} | concatenate | bytes 32768 | tf_op jit(solution)/shard_map/concatenate | solution.py:910
  4.0 108.7 %shard_map.235 = bf16[256,128]{1,0:T(8,128)(2,1)} custom-call(bf16[64,256]{1,0:T(8,128)(2,1)} %bitcast.48, bf16[256,128]{1,0:T(8,128)(2,1)} %wide_in.1, bf16[64,256]{1,0:T(8,128)(2,1)} %bitcast.49, bf16[256,128]{1,0:T(8,128)(2,1)} %wide_gate.1, f32[16,256]{1,0:T(8,128)} %concatenate.3.lines, f32[4,64]{1,0:T(4,128)} %narrow_taps.1, f32[4,128]{1,0:T(4,128)} %wide_taps.1, ...), custom_call_target="tpu_custom_call" | custom-call | tf_op jit(solution)/shard_map/pallas_call | solution.py:815
  112.7 1.5 %copy.29 = bf16[256,128]{1,0:T(8,128)(2,1)} copy(bf16[256,128]{1,0:T(8,128)(2,1)} %shard_map.235) | data formatting | bytes 131072
  (3 shorter events, 0.0 us)
Async XLA Ops:
  0.0 0.7 copy-start.5
  0.0 0.7 copy-start.4
  0.7 0.7 copy-start.2
  0.7 0.7 copy-start.3
  1.4 0.7 copy-start.1
  2.0 0.7 copy-start
